TPU v7x, 32 devices: a whole 2x2x4 slice. The times are simulated.
32 devices in a mesh: sp: 8 (over z, x), tp: 4 (over y, core).
Axes of the slice: x: 2, y: 2, z: 4, core: 2. Of those that a mesh axis runs over, the one named last changes fastest.
Arguments:
- residual: bfloat16 [6144, 2048], P('sp'), may hold values from -6 to 6
- query_matrix: bfloat16 [6144, 1024], P('sp', 'tp'), may hold values from -6 to 6
- key_matrix: bfloat16 [6144, 1024], P('sp', 'tp'), may hold values from -6 to 6
- value_matrix: bfloat16 [6144, 2048], P('sp', 'tp'), may hold values from -6 to 6
- output_gate_logit: bfloat16 [6144, 2048], P('sp', 'tp'), may hold values from -6 to 6
- input_gate_log: float32 [6144, 8], P('sp', 'tp'), may hold values from -4 to 125
- forget_gate_logit: float32 [6144, 8], P('sp', 'tp')
- extra_head_decay: float32 [6144, 8], P('sp', 'tp'), may hold values from -1 to 0
- head_norm_gain: float32 [2048], P('tp'), may hold values from 0.1 to 1.9
- projection: bfloat16 [2048, 2048], P('tp'), may hold values from -5.303301 to 5.303301
- cell_output_gain: float32 [2048], replicated, may hold values from 0.1 to 1.9
- mixer_input_gain: float32 [2048], replicated, may hold values from 0.1 to 1.9
- mixer_gate_weight: bfloat16 [2048, 5120], P('sp', 'tp'), may hold values from -0.125 to 0.125
- mixer_up_weight: bfloat16 [2048, 5120], P('sp', 'tp'), may hold values from -0.125 to 0.125
- mixer_down_weight: bfloat16 [5120, 2048], P('tp', 'sp'), may hold values from -0.078125 to 0.078125
Outputs:
- updated: bfloat16 [6144, 2048], P('sp', 'tp')
All inputs are finite; a program needn't handle non-finite values.
Results may differ from a plain program's by a relative error of at most 0.014.
Values may be sent and summed in bfloat16 or wider, within the bound.
A program may use at most 128 MiB of HBM per device.

v0:
```python
import functools

import jax
import jax.numpy as jnp
from jax import lax
from jax.experimental import pallas as pl
from jax.experimental.pallas import tpu as pltpu
from jax.sharding import PartitionSpec as P

DQK = 128
DV = 256
MESH = pl.DeviceIdType.MESH
VMEM = pl.BlockSpec(memory_space=pltpu.VMEM)
ANY = pl.BlockSpec(memory_space=pl.ANY)
VMEM_BYTES = 62 * 1024 * 1024

HIGHEST = lax.Precision.HIGHEST
EPSILON = 1e-06
LOWEST_LOG = -1e30


def heads_first(array, heads, width):
    return array.reshape(array.shape[0], heads, width).transpose(1, 0, 2)


def fold_state(keyed, valued, in_logs, running_log_total, memory, normalizer, stabilizer):
    last = running_log_total[:, -1]
    lifted = last[:, None] - running_log_total + in_logs
    new_max = jnp.maximum(last + stabilizer, jnp.max(lifted, axis=-1))
    weights = jnp.exp(lifted - new_max[:, None])
    retained = jnp.exp(last + stabilizer - new_max)
    memory = retained[:, None, None] * memory + jnp.einsum(
        "hsv,hsd->hvd", weights[:, :, None] * valued, keyed, precision=HIGHEST
    )
    normalizer = retained[:, None] * normalizer + jnp.einsum(
        "hs,hsd->hd", weights, keyed, precision=HIGHEST
    )
    return (memory, normalizer, new_max)


def copy_to(source, target, sems, slot, peer):
    return pltpu.make_async_remote_copy(
        source, target, sems.at[(0, *slot)], sems.at[(1, *slot)], device_id=peer, device_id_type=MESH
    )


def layer_kernel(
    ranks, count, heads, carried_by_hand, memory_ref, aux_ref, cum_row, in_row, cum_col, query_ref,
    key_ref, value_ref, ogate_ref, head_gain, residual_ref, out_gain, in_gain, projection_ref,
    gate_ref, up_ref, down_ref, out_ref, slots, aux_slots, memory, aux, gate_w, up_w, down_w,
    weight, gated, blocks, normed, first, active, to_core, from_core, to_chip, from_chip,
    state_sems, aux_sems, line_sems, cross_sems, local_sems, proj_sems, gated_sems, sum_sems,
):
    sp, me = lax.axis_index("sp"), lax.axis_index("tp")
    row, col = sp // 2, lax.rem(sp, 2)
    depth = ranks // 2
    core = lax.rem(me, 2)
    mate = me + 1 - 2 * core
    chips = count // 2
    rows_all, width = residual_ref.shape
    cols = out_ref.shape[1]
    inner = value_ref.shape[1]
    pending = []

    barrier = pltpu.get_barrier_semaphore()
    for axis, size, at in (("sp", ranks, sp), ("tp", count, me)):
        for step in range(1, size):
            pl.semaphore_signal(
                barrier, inc=1, device_id={axis: lax.rem(at + step, size)}, device_id_type=MESH
            )
    pl.semaphore_wait(barrier, ranks + count - 2)

    def when(condition, action):
        pl.when(condition)(action)

    def state_copies(step):
        peer = {"sp": lax.rem(sp + step, ranks)}
        return (
            copy_to(memory_ref, slots.at[step - 1], state_sems, (step - 1,), peer),
            copy_to(aux_ref, aux_slots.at[step - 1], aux_sems, (step - 1,), peer),
        )

    for step in range(1, ranks):

        @pl.when(sp + step < ranks)
        def _():
            for copy in state_copies(step):
                copy.start()

    half = down_w.shape[1] // 2
    high = gate_ref.shape[0]

    def views(kind, owner):
        rows = pl.ds(pl.multiple_of(owner * high, high), high)
        if kind == 0:
            return gate_ref, gate_w.at[rows, :]
        if kind == 1:
            return up_ref, up_w.at[rows, :]
        rows = pl.ds(0 if kind == 2 else half, half)
        return down_ref.at[rows, :], down_w.at[owner, rows, :]

    other = 1 - col
    line_slot = lambda way: 1 if way > 0 else 0

    def along(kind, step, column, mine, way):
        owner = (row - step) * 2 + column
        source, target = views(kind, owner)
        if step != 0 or not mine:
            source = target
        slot = (kind, 0 if mine else 1, abs(step), line_slot(way))
        return copy_to(source, target, line_sems, slot, {"sp": sp + 2 * way})

    def across(kind, step):
        owner = (row - step) * 2 + col
        source, target = views(kind, owner)
        if step != 0:
            source = target
        slot = (kind, step + depth - 1)
        return copy_to(source, target, cross_sems, slot, {"sp": row * 2 + other})

    def crossed(kind, step):
        owner = (row - step) * 2 + other
        source, target = views(kind, owner)
        return copy_to(target, target, cross_sems, (kind, step + depth - 1), {"sp": row * 2 + other})

    def came(kind, step, column, mine):
        owner = (row - step) * 2 + column
        source, target = views(kind, owner)
        way = 1 if step > 0 else -1
        slot = (kind, 0 if mine else 1, abs(step) - 1, line_slot(way))
        return copy_to(target, target, line_sems, slot, {"sp": sp})

    def exists(way):
        return jnp.logical_and(row + way >= 0, row + way < depth)

    def send_along(kind, step, column, mine, way):
        def start():
            along(kind, step, column, mine, way).start()

        has = jnp.logical_and(row - step >= 0, row - step < depth)
        when(jnp.logical_and(has, exists(way)), start)
        pending.append((jnp.logical_and(has, exists(way)), along(kind, step, column, mine, way)))

    def send_across(kind, step):
        has = jnp.logical_and(row - step >= 0, row - step < depth)
        when(has, lambda: across(kind, step).start())
        pending.append((has, across(kind, step)))

    def stage(step, kinds):
        for kind in kinds:
            for column, mine in ((col, True), (other, False)):
                if kind < 3 and not mine:
                    continue
                for way in (1, -1):
                    has = jnp.logical_and(row - way * step >= 0, row - way * step < depth)
                    when(has, lambda: came(kind, way * step, column, mine).wait_recv())
                    if step < depth - 1:
                        send_along(kind, way * step, column, mine, way)
                    if kind < 3:
                        send_across(kind, way * step)

    def finish(kinds):
        for kind in kinds:
            steps = range(1 - depth, depth) if kind < 3 else ()
            for step in steps:
                has = jnp.logical_and(row - step >= 0, row - step < depth)
                when(has, lambda: crossed(kind, step).wait_recv())

    def own(kind):
        source, target = views(kind, sp)
        return pltpu.make_async_copy(source, target, local_sems.at[kind])

    def spread(source, whole, sems):
        sent = [copy_to(source, whole.at[me], sems, (0,), {"tp": mate})]
        for step in range(1, chips):
            peer = {"tp": lax.rem(me + 2 * step, count)}
            sent.append(copy_to(source, whole.at[me], sems, (2 * step,), peer))
        for copy in sent:
            copy.start()
        return sent

    def relay(whole, sems):
        sent = []
        for step in range(1, chips):
            owner = lax.rem(me - 2 * step + count, count)
            block = whole.at[owner]
            copy_to(block, block, sems, (2 * step,), {"tp": mate}).wait_recv()
            sent.append(copy_to(block, block, sems, (2 * step - 1,), {"tp": mate}))
            sent[-1].start()
        return sent

    def collect(whole, sems):
        for step in range(chips):
            owner = lax.rem(mate - 2 * step + count, count)
            block = whole.at[owner]
            slot = 0 if step == 0 else 2 * step - 1
            copy_to(block, block, sems, (slot,), {"tp": mate}).wait_recv()

    if carried_by_hand:
        for kind in range(4):
            if kind == 3:
                send_across(3, 0)
            for way in (1, -1):
                send_along(kind, 0, col, True, way)
            if kind < 3:
                send_across(kind, 0)
            own(kind).start()
    else:
        for ref, whole, at in ((gate_ref, gate_w, 0), (up_ref, up_w, 1)):
            pltpu.make_async_copy(ref, whole, local_sems.at[at]).start()
        pltpu.make_async_copy(down_ref, down_w.at[0], local_sems.at[2]).start()
    own_weight = pltpu.make_async_copy(projection_ref, weight.at[me], local_sems.at[4])
    own_weight.start()
    sent = spread(projection_ref, weight, proj_sems)

    memory[...] = jnp.zeros_like(memory)
    aux[...] = jnp.zeros_like(aux)
    aux[heads : 2 * heads, :] = jnp.full((heads, DQK), LOWEST_LOG, jnp.float32)
    for step in range(ranks - 1, 0, -1):

        @pl.when(sp >= step)
        def _():
            for copy in state_copies(step):
                copy.wait_recv()
            late = aux_slots[step - 1]
            for head in range(heads):
                rows = pl.ds(head * DV, DV)
                early_max = aux[heads + head : heads + head + 1, :]
                late_max = late[heads + head : heads + head + 1, :]
                late_decay = late[2 * heads + head : 2 * heads + head + 1, :]
                joined = jnp.maximum(late_decay + early_max, late_max)
                before = jnp.exp(late_decay + early_max - joined)
                after = jnp.exp(late_max - joined)
                memory[rows, :] = before * memory[rows, :] + after * slots[
                    step - 1, rows, :
                ].astype(jnp.float32)
                aux[head : head + 1, :] = (
                    before * aux[head : head + 1, :] + after * late[head : head + 1, :]
                )
                aux[heads + head : heads + head + 1, :] = joined
                aux[2 * heads + head : 2 * heads + head + 1, :] = (
                    aux[2 * heads + head : 2 * heads + head + 1, :] + late_decay
                )

    if carried_by_hand:
        crossed(3, 0).wait_recv()
        for way in (1, -1):
            send_along(3, 0, other, False, way)
        stage(1, (0,))

    tile = rows_all // 3
    for head in range(heads):
        prior_max = aux[heads + head : heads + head + 1, :]
        start_max = jnp.maximum(aux[2 * heads + head : 2 * heads + head + 1, :], prior_max)
        lift = jnp.exp(prior_max - start_max) * DQK ** (-0.5)
        memory[head * DV : (head + 1) * DV, :] = memory[head * DV : (head + 1) * DV, :] * lift
        aux[head : head + 1, :] = aux[head : head + 1, :] * lift
        aux[2 * heads + head : 2 * heads + head + 1, :] = start_max

    def read(at, unused):
        start = pl.multiple_of(at * tile, tile)
        rows = pl.ds(start, tile)
        causal = start + lax.broadcasted_iota(
            jnp.int32, (tile, rows_all), 0
        ) >= lax.broadcasted_iota(jnp.int32, (tile, rows_all), 1)
        for head in range(heads):
            keys = slice(head * DQK, (head + 1) * DQK)
            values = slice(head * DV, (head + 1) * DV)
            query = query_ref[rows, keys]
            total = cum_col[rows, head : head + 1]
            spread_log = total - cum_row[head : head + 1, :] + in_row[head : head + 1, :]
            spread_log = jnp.where(causal, spread_log, -jnp.inf)
            carried = total + aux[2 * heads + head : 2 * heads + head + 1, :1]
            running = jnp.maximum(carried, jnp.max(spread_log, axis=-1, keepdims=True))
            scores = lax.dot_general(
                query, key_ref[:, keys], (((1,), (1,)), ((), ())),
                preferred_element_type=jnp.float32,
            ) * DQK ** (-0.5)
            weights = jnp.exp(spread_log - running) * scores
            scaled = jnp.exp(carried - running)
            wide = query.astype(jnp.float32)
            numerator = jnp.dot(
                weights.astype(jnp.bfloat16), value_ref[:, values],
                preferred_element_type=jnp.float32,
            ) + scaled * lax.dot_general(
                wide, memory[values, :], (((1,), (1,)), ((), ())), precision=HIGHEST,
                preferred_element_type=jnp.float32,
            )
            denominator = jnp.sum(weights, axis=-1, keepdims=True) + scaled * jnp.sum(
                wide * aux[head : head + 1, :], axis=-1, keepdims=True
            )
            cell = numerator / jnp.maximum(jnp.abs(denominator), jnp.exp(-running))
            centered = cell - jnp.mean(cell, axis=-1, keepdims=True)
            cell = centered * lax.rsqrt(
                jnp.mean(centered * centered, axis=-1, keepdims=True) + EPSILON
            )
            cell = cell * head_gain[:, values]
            gate = ogate_ref[rows, values].astype(jnp.float32)
            gated[rows, values] = (cell * jax.nn.sigmoid(gate)).astype(jnp.bfloat16)
        return unused

    lax.fori_loop(0, 3, read, 0)
    sent += spread(gated, blocks, gated_sems)
    blocks[me] = gated[...]
    if carried_by_hand:
        stage(1, (1, 2, 3))
    sent += relay(weight, proj_sems)
    if carried_by_hand:
        stage(2, (0, 1))
    sent += relay(blocks, gated_sems)
    collect(weight, proj_sems)
    own_weight.wait()
    collect(blocks, gated_sems)

    def turn(at, unused):
        rows = pl.ds(pl.multiple_of(at * tile, tile), tile)
        mixed = jnp.zeros((tile, width), jnp.float32)
        for block in range(count):
            mixed = mixed + jnp.dot(
                blocks[block, rows, :], weight[block], preferred_element_type=jnp.float32
            )
        scale = lax.rsqrt(jnp.mean(mixed * mixed, axis=-1, keepdims=True) + EPSILON)
        total = residual_ref[rows, :].astype(jnp.float32) + mixed * scale * out_gain[...]
        total = total.astype(jnp.bfloat16)
        first[rows, :] = total
        wide = total.astype(jnp.float32)
        scale = lax.rsqrt(jnp.mean(wide * wide, axis=-1, keepdims=True) + EPSILON)
        normed[rows, :] = (wide * scale * in_gain[...]).astype(jnp.bfloat16)
        return unused

    lax.fori_loop(0, 3, turn, 0)

    if carried_by_hand:
        stage(2, (2, 3))
        stage(3, (0, 1, 2))
        finish((0, 1))
        own(0).wait()
        own(1).wait()
    else:
        for ref, whole, at in ((gate_ref, gate_w, 0), (up_ref, up_w, 1)):
            pltpu.make_async_copy(ref, whole, local_sems.at[at]).wait()

    def mix(at, unused):
        rows = pl.ds(pl.multiple_of(at * tile, tile), tile)
        left = normed[rows, :]
        gate = jnp.dot(left, gate_w[...], preferred_element_type=jnp.float32)
        up = jnp.dot(left, up_w[...], preferred_element_type=jnp.float32)
        active[rows, :] = (gate / (1.0 + jnp.exp(-gate)) * up).astype(jnp.bfloat16)
        return unused

    lax.fori_loop(0, 3, mix, 0)
    if carried_by_hand:
        stage(3, (3,))
        finish((2, 3))
        own(2).wait()
        own(3).wait()
    else:
        pltpu.make_async_copy(down_ref, down_w.at[0], local_sems.at[2]).wait()

    def term(target):
        if carried_by_hand:
            each = cols // down_w.shape[2]
            return jnp.concatenate(
                [
                    jnp.dot(active[...], down_w[target * each + at],
                            preferred_element_type=jnp.float32)
                    for at in range(each)
                ],
                axis=1,
            )
        start = pl.multiple_of(target * cols, cols)
        return jnp.dot(
            active[...], down_w[0, :, pl.ds(start, cols)], preferred_element_type=jnp.float32
        )

    def send(source, target, kind, at, peer):
        return copy_to(source.at[at], target.at[at], sum_sems.at[kind], (at,), {"tp": peer})

    copies = []
    for step in range(1, chips):
        away = lax.rem(me + 2 * step, count)
        to_core[step] = term(away + 1 - 2 * core).astype(jnp.bfloat16)
        hop = send(to_core, from_core, 0, step, mate)
        hop.start()
        mine = term(away)
        hop.wait_recv()
        to_chip[step] = (mine + from_core[step].astype(jnp.float32)).astype(jnp.bfloat16)
        far = send(to_chip, from_chip, 1, step, away)
        far.start()
        copies += [hop, far]
    to_core[0] = term(mate).astype(jnp.bfloat16)
    hop = send(to_core, from_core, 0, 0, mate)
    hop.start()
    result = term(me)
    hop.wait_recv()
    result = result + from_core[0].astype(jnp.float32)
    for far in copies[1::2]:
        far.wait_recv()
    for step in range(1, chips):
        result = result + from_chip[step].astype(jnp.float32)
    own_first = first[:, pl.ds(pl.multiple_of(me * cols, cols), cols)]
    out_ref[...] = (own_first.astype(jnp.float32) + 0.5 * result).astype(jnp.bfloat16)
    for copy in copies + [hop] + sent:
        copy.wait_send()
    for condition, copy in pending:
        when(condition, copy.wait_send)
    for step in range(1, ranks):

        @pl.when(sp + step < ranks)
        def _():
            for copy in state_copies(step):
                copy.wait_send()


def layer(states, logs, cell_inputs, residual, gains, weights):
    decay, memory, normalizer, maximum = states
    running_log_total, in_logs = logs
    ranks, count = lax.axis_size("sp"), lax.axis_size("tp")
    heads = decay.shape[0]
    rows, width = residual.shape
    projection, gate_weight, up_weight, down_weight = weights
    hidden = gate_weight.shape[1]
    inner = projection.shape[0]
    carried_by_hand = ranks == 8
    if carried_by_hand:
        down_shape = (ranks, hidden, down_weight.shape[1])
    else:
        gate_weight = lax.all_gather(gate_weight, "sp", axis=0, tiled=True)
        up_weight = lax.all_gather(up_weight, "sp", axis=0, tiled=True)
        down_weight = lax.all_gather(down_weight, "sp", axis=1, tiled=True)
        down_shape = (1, hidden, width)
    fill = lambda row: jnp.broadcast_to(row[:, None], (heads, DQK))
    aux = jnp.concatenate([normalizer, fill(maximum), fill(decay)])
    height = -(-3 * heads // 8) * 8
    aux = jnp.pad(aux, ((0, height - 3 * heads), (0, 0)))
    low = memory.reshape(heads * DV, DQK).astype(jnp.bfloat16)
    chips, cols, depth = count // 2, width // count, ranks // 2
    buffer = pltpu.VMEM((chips, rows, cols), jnp.bfloat16)
    dma = pltpu.SemaphoreType.DMA
    return pl.pallas_call(
        functools.partial(layer_kernel, ranks, count, heads, carried_by_hand),
        out_shape=jax.ShapeDtypeStruct((rows, cols), jnp.bfloat16),
        in_specs=[VMEM] * 13 + [ANY] * 4,
        out_specs=VMEM,
        scratch_shapes=[
            pltpu.VMEM((ranks - 1, heads * DV, DQK), jnp.bfloat16),
            pltpu.VMEM((ranks - 1, height, DQK), jnp.float32),
            pltpu.VMEM((heads * DV, DQK), jnp.float32),
            pltpu.VMEM((height, DQK), jnp.float32),
            pltpu.VMEM((width, hidden), jnp.bfloat16),
            pltpu.VMEM((width, hidden), jnp.bfloat16),
            pltpu.VMEM(down_shape, jnp.bfloat16),
            pltpu.VMEM((count, inner, width), jnp.bfloat16),
            pltpu.VMEM((rows, inner), jnp.bfloat16),
            pltpu.VMEM((count, rows, inner), jnp.bfloat16),
            pltpu.VMEM((rows, width), jnp.bfloat16),
            pltpu.VMEM((rows, width), jnp.bfloat16),
            pltpu.VMEM((rows, hidden), jnp.bfloat16),
            buffer, buffer, buffer, buffer,
            dma((2, ranks - 1)),
            dma((2, ranks - 1)),
            dma((2, 4, 2, depth, 2)),
            dma((2, 4, 2 * depth - 1)),
            dma((5,)),
            dma((2, count)),
            dma((2, count)),
            dma((2, 2, chips)),
        ],
        compiler_params=pltpu.CompilerParams(
            collective_id=0, has_side_effects=True, vmem_limit_bytes=VMEM_BYTES
        ),
        name="layer",
    )(
        low, aux, running_log_total, in_logs, running_log_total.T, *cell_inputs, residual,
        *gains, projection, gate_weight, up_weight, down_weight,
    )


def body(
    residual,
    query_matrix,
    key_matrix,
    value_matrix,
    output_gate_logit,
    input_gate_log,
    forget_gate_logit,
    extra_head_decay,
    head_norm_gain,
    projection,
    cell_output_gain,
    mixer_input_gain,
    mixer_gate_weight,
    mixer_up_weight,
    mixer_down_weight,
):
    heads_here = input_gate_log.shape[1]
    key_low = heads_first(key_matrix, heads_here, DQK)
    value_low = heads_first(value_matrix, heads_here, DV)
    keyed = key_low.astype(jnp.float32)
    valued = value_low.astype(jnp.float32)
    in_logs = input_gate_log.T
    running_log_total = jnp.cumsum(
        (jax.nn.log_sigmoid(forget_gate_logit) + extra_head_decay).T, axis=-1
    )
    zero_memory = jnp.zeros((heads_here, DV, DQK), jnp.float32)
    zero_normalizer = jnp.zeros((heads_here, DQK), jnp.float32)
    lowest = jnp.full((heads_here,), LOWEST_LOG, jnp.float32)
    local_memory, local_normalizer, local_max = fold_state(
        keyed, valued, in_logs, running_log_total, zero_memory, zero_normalizer, lowest
    )
    return layer(
        (running_log_total[:, -1], local_memory, local_normalizer, local_max),
        (running_log_total, in_logs),
        (query_matrix, key_matrix, value_matrix, output_gate_logit, head_norm_gain[None]),
        residual,
        (cell_output_gain[None], mixer_input_gain[None]),
        (projection, mixer_gate_weight, mixer_up_weight, mixer_down_weight),
    )


def solution(mesh):
    return jax.shard_map(
        body,
        mesh=mesh,
        in_specs=(
            P("sp", None),
            P("sp", "tp"),
            P("sp", "tp"),
            P("sp", "tp"),
            P("sp", "tp"),
            P("sp", "tp"),
            P("sp", "tp"),
            P("sp", "tp"),
            P("tp"),
            P("tp", None),
            P(),
            P(),
            P("sp", "tp"),
            P("sp", "tp"),
            P("tp", "sp"),
        ),
        out_specs=P("sp", "tp"),
        check_vma=False,
    )
```

profile of v0, /device:TPU:25, one launch (start us, length us, event | category | flops | bytes accessed | tf_op | source)
XLA Modules:
  0.0 211.9 jit_solution(3730808388254791454)
XLA Ops:
  0.0 0.7 fusion.15
  0.8 0.6 reduce-window.6
  1.3 0.2 slice_reduce_fusion
  1.5 0.2 reduce-window.9
  1.7 0.1 broadcast_add_fusion
  1.8 0.2 copy.23
  1.9 0.0 copy-start
  2.0 0.1 pad.7.clone
  2.0 0.7 copy.28.cum_row
  2.8 0.9 copy.24
  3.7 0.1 fusion.12
  3.9 0.1 pad.6.clone
  3.9 0.7 copy.29.in_row
  4.7 0.1 subtract_exponential_fusion
  4.8 0.1 copy.30
  4.9 0.3 fusion.9
  5.2 0.1 broadcast_add_fusion.1
  5.3 0.1 maximum_maximum_fusion
  5.3 0.6 pad.4.aux_ref
  6.0 0.1 copy.25
  6.1 0.3 copy.32
  6.4 1.5 fusion.5
  7.9 201.9 %layer.1 = bf16[768,512]{1,0:T(8,128)(2,1)} custom-call(bf16[512,128]{1,0:T(8,128)(2,1)} %bitcast.59, f32[8,128]{1,0:T(8,128)} %pad.4.aux_ref, f32[2,768]{1,0:T(2,128)} %copy.28.cum_row, f32[2,768]{1,0:T(2,128)} %copy.29.in_row, f32[768,2]{1,0:T(8,128)} %bitcast.55, bf16[768,256]{1,0:T(8,128)(2,1)} %query_ref.1, bf16[768,256]{1,0:T(8,128)(2,1)} %key_ref.1, ...), custom_call_target="tpu_custom_call" | custom-call | tf_op jit(solution)/shard_map/layer/pallas_call | solution.py:440
  209.9 2.1 copy.43
  (9 shorter events, 0.0 us)
Async XLA Ops:
  1.9 2.8 %copy-start = (f32[2,6,128]{0,2,1:T(8,128)}, f32[2,6,128]{0,2,1:T(8,128)S(1)}, u32[]{:S(2)}) copy-start(f32[2,6,128]{0,2,1:T(8,128)S(1)} %copy.23) | copy-start | bytes 18436
  2.8 2.1 %copy-start.1 = (bf16[768,256]{1,0:T(8,128)(2,1)S(1)}, bf16[768,256]{1,0:T(8,128)(2,1)}, u32[]{:S(2)}) copy-start(bf16[768,256]{1,0:T(8,128)(2,1)} %key_ref.1) | copy-start | bytes 1179652
  3.8 2.3 %copy-start.2 = (bf16[768,512]{1,0:T(8,128)(2,1)S(1)}, bf16[768,512]{1,0:T(8,128)(2,1)}, u32[]{:S(2)}) copy-start(bf16[768,512]{1,0:T(8,128)(2,1)} %value_ref.1) | copy-start | bytes 2359300
where the time goes:
time: 212 us
  Pallas kernels  202 us (95%)
  local copies, waits for them, and re-layouts  6.18 us (3%)
    pallas_call x1, Pallas kernels, layer(): pl.pallas_call(functools.partial(layer_kernel, ranks, count, heads, carri...  202 us

commit v1 on v0

--- a/solution.py
+++ b/solution.py
@@ -45,22 +45,19 @@
 
 
 def layer_kernel(
-    ranks, count, heads, carried_by_hand, memory_ref, aux_ref, cum_row, in_row, cum_col, query_ref,
+    ranks, count, heads, memory_ref, aux_ref, cum_row, in_row, cum_col, query_ref,
     key_ref, value_ref, ogate_ref, head_gain, residual_ref, out_gain, in_gain, projection_ref,
     gate_ref, up_ref, down_ref, out_ref, slots, aux_slots, memory, aux, gate_w, up_w, down_w,
     weight, gated, blocks, normed, first, active, to_core, from_core, to_chip, from_chip,
-    state_sems, aux_sems, line_sems, cross_sems, local_sems, proj_sems, gated_sems, sum_sems,
+    state_sems, aux_sems, local_sems, proj_sems, gated_sems, sum_sems,
 ):
     sp, me = lax.axis_index("sp"), lax.axis_index("tp")
-    row, col = sp // 2, lax.rem(sp, 2)
-    depth = ranks // 2
     core = lax.rem(me, 2)
     mate = me + 1 - 2 * core
     chips = count // 2
     rows_all, width = residual_ref.shape
     cols = out_ref.shape[1]
     inner = value_ref.shape[1]
-    pending = []
 
     barrier = pltpu.get_barrier_semaphore()
     for axis, size, at in (("sp", ranks, sp), ("tp", count, me)):
@@ -70,9 +67,6 @@
             )
     pl.semaphore_wait(barrier, ranks + count - 2)
 
-    def when(condition, action):
-        pl.when(condition)(action)
-
     def state_copies(step):
         peer = {"sp": lax.rem(sp + step, ranks)}
         return (
@@ -86,89 +80,6 @@
         def _():
             for copy in state_copies(step):
                 copy.start()
-
-    half = down_w.shape[1] // 2
-    high = gate_ref.shape[0]
-
-    def views(kind, owner):
-        rows = pl.ds(pl.multiple_of(owner * high, high), high)
-        if kind == 0:
-            return gate_ref, gate_w.at[rows, :]
-        if kind == 1:
-            return up_ref, up_w.at[rows, :]
-        rows = pl.ds(0 if kind == 2 else half, half)
-        return down_ref.at[rows, :], down_w.at[owner, rows, :]
-
-    other = 1 - col
-    line_slot = lambda way: 1 if way > 0 else 0
-
-    def along(kind, step, column, mine, way):
-        owner = (row - step) * 2 + column
-        source, target = views(kind, owner)
-        if step != 0 or not mine:
-            source = target
-        slot = (kind, 0 if mine else 1, abs(step), line_slot(way))
-        return copy_to(source, target, line_sems, slot, {"sp": sp + 2 * way})
-
-    def across(kind, step):
-        owner = (row - step) * 2 + col
-        source, target = views(kind, owner)
-        if step != 0:
-            source = target
-        slot = (kind, step + depth - 1)
-        return copy_to(source, target, cross_sems, slot, {"sp": row * 2 + other})
-
-    def crossed(kind, step):
-        owner = (row - step) * 2 + other
-        source, target = views(kind, owner)
-        return copy_to(target, target, cross_sems, (kind, step + depth - 1), {"sp": row * 2 + other})
-
-    def came(kind, step, column, mine):
-        owner = (row - step) * 2 + column
-        source, target = views(kind, owner)
-        way = 1 if step > 0 else -1
-        slot = (kind, 0 if mine else 1, abs(step) - 1, line_slot(way))
-        return copy_to(target, target, line_sems, slot, {"sp": sp})
-
-    def exists(way):
-        return jnp.logical_and(row + way >= 0, row + way < depth)
-
-    def send_along(kind, step, column, mine, way):
-        def start():
-            along(kind, step, column, mine, way).start()
-
-        has = jnp.logical_and(row - step >= 0, row - step < depth)
-        when(jnp.logical_and(has, exists(way)), start)
-        pending.append((jnp.logical_and(has, exists(way)), along(kind, step, column, mine, way)))
-
-    def send_across(kind, step):
-        has = jnp.logical_and(row - step >= 0, row - step < depth)
-        when(has, lambda: across(kind, step).start())
-        pending.append((has, across(kind, step)))
-
-    def stage(step, kinds):
-        for kind in kinds:
-            for column, mine in ((col, True), (other, False)):
-                if kind < 3 and not mine:
-                    continue
-                for way in (1, -1):
-                    has = jnp.logical_and(row - way * step >= 0, row - way * step < depth)
-                    when(has, lambda: came(kind, way * step, column, mine).wait_recv())
-                    if step < depth - 1:
-                        send_along(kind, way * step, column, mine, way)
-                    if kind < 3:
-                        send_across(kind, way * step)
-
-    def finish(kinds):
-        for kind in kinds:
-            steps = range(1 - depth, depth) if kind < 3 else ()
-            for step in steps:
-                has = jnp.logical_and(row - step >= 0, row - step < depth)
-                when(has, lambda: crossed(kind, step).wait_recv())
-
-    def own(kind):
-        source, target = views(kind, sp)
-        return pltpu.make_async_copy(source, target, local_sems.at[kind])
 
     def spread(source, whole, sems):
         sent = [copy_to(source, whole.at[me], sems, (0,), {"tp": mate})]
@@ -196,19 +107,9 @@
             slot = 0 if step == 0 else 2 * step - 1
             copy_to(block, block, sems, (slot,), {"tp": mate}).wait_recv()
 
-    if carried_by_hand:
-        for kind in range(4):
-            if kind == 3:
-                send_across(3, 0)
-            for way in (1, -1):
-                send_along(kind, 0, col, True, way)
-            if kind < 3:
-                send_across(kind, 0)
-            own(kind).start()
-    else:
-        for ref, whole, at in ((gate_ref, gate_w, 0), (up_ref, up_w, 1)):
-            pltpu.make_async_copy(ref, whole, local_sems.at[at]).start()
-        pltpu.make_async_copy(down_ref, down_w.at[0], local_sems.at[2]).start()
+    for ref, whole, at in ((gate_ref, gate_w, 0), (up_ref, up_w, 1)):
+        pltpu.make_async_copy(ref, whole, local_sems.at[at]).start()
+    pltpu.make_async_copy(down_ref, down_w.at[0], local_sems.at[2]).start()
     own_weight = pltpu.make_async_copy(projection_ref, weight.at[me], local_sems.at[4])
     own_weight.start()
     sent = spread(projection_ref, weight, proj_sems)
@@ -241,12 +142,6 @@
                 aux[2 * heads + head : 2 * heads + head + 1, :] = (
                     aux[2 * heads + head : 2 * heads + head + 1, :] + late_decay
                 )
-
-    if carried_by_hand:
-        crossed(3, 0).wait_recv()
-        for way in (1, -1):
-            send_along(3, 0, other, False, way)
-        stage(1, (0,))
 
     tile = rows_all // 3
     for head in range(heads):
@@ -302,11 +197,7 @@
     lax.fori_loop(0, 3, read, 0)
     sent += spread(gated, blocks, gated_sems)
     blocks[me] = gated[...]
-    if carried_by_hand:
-        stage(1, (1, 2, 3))
     sent += relay(weight, proj_sems)
-    if carried_by_hand:
-        stage(2, (0, 1))
     sent += relay(blocks, gated_sems)
     collect(weight, proj_sems)
     own_weight.wait()
@@ -330,15 +221,8 @@
 
     lax.fori_loop(0, 3, turn, 0)
 
-    if carried_by_hand:
-        stage(2, (2, 3))
-        stage(3, (0, 1, 2))
-        finish((0, 1))
-        own(0).wait()
-        own(1).wait()
-    else:
-        for ref, whole, at in ((gate_ref, gate_w, 0), (up_ref, up_w, 1)):
-            pltpu.make_async_copy(ref, whole, local_sems.at[at]).wait()
+    for ref, whole, at in ((gate_ref, gate_w, 0), (up_ref, up_w, 1)):
+        pltpu.make_async_copy(ref, whole, local_sems.at[at]).wait()
 
     def mix(at, unused):
         rows = pl.ds(pl.multiple_of(at * tile, tile), tile)
@@ -349,25 +233,9 @@
         return unused
 
     lax.fori_loop(0, 3, mix, 0)
-    if carried_by_hand:
-        stage(3, (3,))
-        finish((2, 3))
-        own(2).wait()
-        own(3).wait()
-    else:
-        pltpu.make_async_copy(down_ref, down_w.at[0], local_sems.at[2]).wait()
+    pltpu.make_async_copy(down_ref, down_w.at[0], local_sems.at[2]).wait()
 
     def term(target):
-        if carried_by_hand:
-            each = cols // down_w.shape[2]
-            return jnp.concatenate(
-                [
-                    jnp.dot(active[...], down_w[target * each + at],
-                            preferred_element_type=jnp.float32)
-                    for at in range(each)
-                ],
-                axis=1,
-            )
         start = pl.multiple_of(target * cols, cols)
         return jnp.dot(
             active[...], down_w[0, :, pl.ds(start, cols)], preferred_element_type=jnp.float32
@@ -402,8 +270,6 @@
     out_ref[...] = (own_first.astype(jnp.float32) + 0.5 * result).astype(jnp.bfloat16)
     for copy in copies + [hop] + sent:
         copy.wait_send()
-    for condition, copy in pending:
-        when(condition, copy.wait_send)
     for step in range(1, ranks):
 
         @pl.when(sp + step < ranks)
@@ -421,24 +287,20 @@
     projection, gate_weight, up_weight, down_weight = weights
     hidden = gate_weight.shape[1]
     inner = projection.shape[0]
-    carried_by_hand = ranks == 8
-    if carried_by_hand:
-        down_shape = (ranks, hidden, down_weight.shape[1])
-    else:
-        gate_weight = lax.all_gather(gate_weight, "sp", axis=0, tiled=True)
-        up_weight = lax.all_gather(up_weight, "sp", axis=0, tiled=True)
-        down_weight = lax.all_gather(down_weight, "sp", axis=1, tiled=True)
-        down_shape = (1, hidden, width)
+    gate_weight = lax.all_gather(gate_weight, "sp", axis=0, tiled=True)
+    up_weight = lax.all_gather(up_weight, "sp", axis=0, tiled=True)
+    down_weight = lax.all_gather(down_weight, "sp", axis=1, tiled=True)
+    down_shape = (1, hidden, width)
     fill = lambda row: jnp.broadcast_to(row[:, None], (heads, DQK))
     aux = jnp.concatenate([normalizer, fill(maximum), fill(decay)])
     height = -(-3 * heads // 8) * 8
     aux = jnp.pad(aux, ((0, height - 3 * heads), (0, 0)))
     low = memory.reshape(heads * DV, DQK).astype(jnp.bfloat16)
-    chips, cols, depth = count // 2, width // count, ranks // 2
+    chips, cols = count // 2, width // count
     buffer = pltpu.VMEM((chips, rows, cols), jnp.bfloat16)
     dma = pltpu.SemaphoreType.DMA
     return pl.pallas_call(
-        functools.partial(layer_kernel, ranks, count, heads, carried_by_hand),
+        functools.partial(layer_kernel, ranks, count, heads),
         out_shape=jax.ShapeDtypeStruct((rows, cols), jnp.bfloat16),
         in_specs=[VMEM] * 13 + [ANY] * 4,
         out_specs=VMEM,
@@ -459,8 +321,6 @@
             buffer, buffer, buffer, buffer,
             dma((2, ranks - 1)),
             dma((2, ranks - 1)),
-            dma((2, 4, 2, depth, 2)),
-            dma((2, 4, 2 * depth - 1)),
             dma((5,)),
             dma((2, count)),
             dma((2, count)),
@@ -474,6 +334,551 @@
         low, aux, running_log_total, in_logs, running_log_total.T, *cell_inputs, residual,
         *gains, projection, gate_weight, up_weight, down_weight,
     )
+
+
+def pair_kernel(
+    ranks, count, heads, forget_hbm, extra_hbm, in_hbm, query_hbm, key_hbm, value_hbm, ogate_hbm,
+    head_gain_hbm, residual_hbm, out_gain_hbm, in_gain_hbm, projection_hbm, gate_hbm, up_hbm,
+    down_hbm, out_ref, forget, extra, in_row, query, key, value, ogate, head_gain, residual,
+    out_gain, in_gain, proj_own, proj_mate, gate_w, up_w, down_w, cum_row, cols, own_mem, mem_send,
+    aux, x_mem, x_aux, e_mem, e_aux, t_mem, t_aux, z_mem, z_aux, p_mem, p_aux, q_mem, q_aux,
+    final_mem, final_aux, local, gated, mate_gated, part_send, part_recv, acc, first_own,
+    first_cols, normed, active, to_core, from_core, y_send, y_recv, z_send, z_recv, held, kept,
+    local_sems, w_sems, state_sems, line_sems, mate_sems, part_sems, ag_sems, first_sems,
+    core_sems, link_sems,
+):
+    sp, me = lax.axis_index("sp"), lax.axis_index("tp")
+    row, col = sp // 2, lax.rem(sp, 2)
+    depth = ranks // 2
+    par = lax.rem(row, 2)
+    core = lax.rem(me, 2)
+    chip = me // 2
+    mate = me + 1 - 2 * core
+    across = lax.rem(me + 2, count)
+    corner = lax.rem(mate + 2, count)
+    rows_all, width = out_ref.shape[0], out_gain.shape[1]
+    cols_out = out_ref.shape[1]
+    block = rows_all // count
+    half = gate_w.shape[1]
+    high = gate_hbm.shape[0]
+    others = {1: row + 1 - 2 * par, 2: lax.rem(row + 2, depth), 3: depth - 1 - row}
+    to_x = {"sp": row * 2 + 1 - col}
+    to_z = {"sp": others[1] * 2 + col}
+    to_mate, to_y = {"tp": mate}, {"tp": across}
+    sent = []
+
+    barrier = pltpu.get_barrier_semaphore()
+    greeted = [{"sp": others[i] * 2 + col} for i in (1, 2, 3)]
+    greeted += [to_x, to_mate, to_y, {"tp": corner}]
+    for peer in greeted:
+        pl.semaphore_signal(barrier, inc=1, device_id=peer, device_id_type=MESH)
+
+    loads = {}
+
+    def load(name, source, target):
+        loads[name] = pltpu.make_async_copy(source, target, local_sems.at[len(loads)])
+        loads[name].start()
+
+    load("forget", forget_hbm, forget)
+    load("extra", extra_hbm, extra)
+    load("in", in_hbm, in_row)
+    load("key", key_hbm, key)
+    load("value", value_hbm, value)
+    load("query", query_hbm, query)
+    load("ogate", ogate_hbm, ogate)
+    load("head", head_gain_hbm, head_gain)
+    load("proj", projection_hbm, proj_own)
+    own_rows = pl.ds(pl.multiple_of(me * block, block), block)
+    load("residual", residual_hbm.at[own_rows, :], residual)
+    load("outg", out_gain_hbm, out_gain)
+    load("ing", in_gain_hbm, in_gain)
+
+    def piece(kind, parity):
+        at = pl.ds(pl.multiple_of(parity * half, half), half)
+        if kind == 2:
+            return down_hbm.at[at, :]
+        return (gate_hbm, up_hbm)[kind].at[:, at]
+
+    def place(kind, owner):
+        if kind == 2:
+            return down_w.at[owner]
+        at = pl.ds(pl.multiple_of(owner * high, high), high)
+        return (gate_w, up_w)[kind].at[at, :]
+
+    for kind in range(3):
+        load(kind, piece(kind, par), place(kind, sp))
+
+    pl.semaphore_wait(barrier, len(greeted))
+
+    def send(source, target, sems, slot, peer):
+        copy = copy_to(source, target, sems, slot, peer)
+        copy.start()
+        sent.append(copy)
+
+    def arrived(target, sems, slot):
+        copy_to(target, target, sems, slot, to_mate).wait_recv()
+
+    def z_weights(kind, i):
+        there = others[i]
+        send(
+            piece(kind, lax.rem(there, 2)), place(kind, sp), w_sems, (kind, 0, i),
+            {"sp": there * 2 + col},
+        )
+
+    def x_weights(kind):
+        send(piece(kind, par), place(kind, sp), w_sems, (kind, 1, 0), to_x)
+
+    relays = [(kind, i) for kind in range(3) for i in (1, 3, 2)]
+
+    def pump(number):
+        for _ in range(number):
+            kind, i = relays.pop(0)
+            spot = place(kind, others[i] * 2 + col)
+            arrived(spot, w_sems, (kind, 0, i))
+            send(spot, spot, w_sems, (kind, 1, i), to_x)
+
+    def gathered(kind):
+        loads[kind].wait()
+        for i in range(depth):
+            there = row if i == 0 else others[i]
+            arrived(place(kind, there * 2 + 1 - col), w_sems, (kind, 1, i))
+
+    z_weights(0, 1)
+    send(projection_hbm, proj_mate, mate_sems, (2,), to_mate)
+
+    for name in ("forget", "extra", "in"):
+        loads[name].wait()
+    logit = forget[...]
+    decay = jnp.minimum(logit, 0.0) - jnp.log1p(jnp.exp(-jnp.abs(logit))) + extra[...]
+    lane = lax.broadcasted_iota(jnp.int32, decay.shape, 1)
+    shift = 1
+    while shift < rows_all:
+        decay = decay + jnp.where(lane >= shift, pltpu.roll(decay, shift, 1), 0.0)
+        shift *= 2
+    cum_row[...] = decay
+    last = decay[:, rows_all - 1 : rows_all]
+    lifted = last - decay + in_row[...]
+    top = jnp.max(lifted, axis=-1, keepdims=True)
+    lifted = jnp.exp(lifted - top)
+    eye = lax.broadcasted_iota(jnp.int32, (128, 128), 0) == lax.broadcasted_iota(
+        jnp.int32, (128, 128), 1
+    )
+
+    def to_column(line, at):
+        for start in range(0, rows_all, 128):
+            spread = jnp.broadcast_to(line[:, start : start + 128], (128, 128))
+            cols[start : start + 128, at : at + 1] = jnp.sum(
+                jnp.where(eye, spread, 0.0), axis=-1, keepdims=True
+            )
+
+    for head in range(heads):
+        to_column(decay[head : head + 1, :], head)
+        to_column(lifted[head : head + 1, :], heads + head)
+    loads["key"].wait()
+    loads["value"].wait()
+    for head in range(heads):
+        keys = slice(head * DQK, (head + 1) * DQK)
+        values = slice(head * DV, (head + 1) * DV)
+        share = cols[:, heads + head : heads + head + 1]
+        heavy = (share * value[:, values].astype(jnp.float32)).astype(jnp.bfloat16)
+        state = lax.dot_general(
+            key[:, keys], heavy, (((0,), (0,)), ((), ())), preferred_element_type=jnp.float32
+        )
+        own_mem[head] = state
+        mem_send[head] = state.astype(jnp.bfloat16)
+        aux[head] = jnp.zeros((8, DQK), jnp.float32)
+        aux[head, 0:1, :] = jnp.sum(
+            share * key[:, keys].astype(jnp.float32), axis=0, keepdims=True
+        )
+        aux[head, 1:2, :] = jnp.broadcast_to(top[head : head + 1, :], (1, DQK))
+        aux[head, 2:3, :] = jnp.broadcast_to(last[head : head + 1, :], (1, DQK))
+    send(mem_send.at[1 - col], x_mem, state_sems, (0,), to_x)
+    send(aux.at[1 - col], x_aux, state_sems, (1,), to_x)
+    x_weights(0)
+
+    tile = rows_all // 3
+    loads["query"].wait()
+
+    def nearby(head, at):
+        start, reach = at * tile, (at + 1) * tile
+        keys = slice(head * DQK, (head + 1) * DQK)
+        values = slice(head * DV, (head + 1) * DV)
+        rows = slice(start, reach)
+        causal = start + lax.broadcasted_iota(
+            jnp.int32, (tile, reach), 0
+        ) >= lax.broadcasted_iota(jnp.int32, (tile, reach), 1)
+        total = cols[rows, head : head + 1]
+        spread_log = total - cum_row[head : head + 1, :reach] + in_row[head : head + 1, :reach]
+        spread_log = jnp.where(causal, spread_log, -jnp.inf)
+        running = jnp.max(spread_log, axis=-1, keepdims=True)
+        scores = lax.dot_general(
+            query[rows, keys], key[:reach, keys], (((1,), (1,)), ((), ())),
+            preferred_element_type=jnp.float32,
+        ) * DQK ** (-0.5)
+        weights = jnp.exp(spread_log - running) * scores
+        local[rows, values] = jnp.dot(
+            weights.astype(jnp.bfloat16), value[:reach, values],
+            preferred_element_type=jnp.float32,
+        )
+        cols[rows, 2 * heads + head : 2 * heads + head + 1] = running
+        cols[rows, 3 * heads + head : 3 * heads + head + 1] = jnp.sum(
+            weights, axis=-1, keepdims=True
+        )
+
+    nearby(0, 0)
+    nearby(1, 0)
+    nearby(0, 1)
+
+    def parts(ref):
+        return ref[0:1, :], ref[1:2, :], ref[2:3, :]
+
+    def join(early_mem, early, late_mem, late):
+        joined = jnp.maximum(late[2] + early[1], late[1])
+        before = jnp.exp(late[2] + early[1] - joined)
+        after = jnp.exp(late[1] - joined)
+        memory = before[:, :1] * early_mem + after[:, :1] * late_mem
+        return memory, (before * early[0] + after * late[0], joined, early[2] + late[2])
+
+    def keep(ref, values):
+        ref[...] = jnp.zeros(ref.shape, jnp.float32)
+        for at, entry in enumerate(values):
+            ref[at : at + 1, :] = entry
+
+    left = col == 0
+    arrived(x_mem, state_sems, (0,))
+    arrived(x_aux, state_sems, (1,))
+    mine, theirs = own_mem[col], x_mem[...].astype(jnp.float32)
+    mine_aux = tuple(aux[col, at : at + 1, :] for at in range(3))
+    theirs_aux = parts(x_aux)
+    pick = lambda one, two: jnp.where(left, one, two)
+    early_mem, late_mem = pick(mine, theirs), pick(theirs, mine)
+    early_aux = tuple(pick(one, two) for one, two in zip(mine_aux, theirs_aux))
+    late_aux = tuple(pick(two, one) for one, two in zip(mine_aux, theirs_aux))
+    e_mem[...] = early_mem
+    keep(e_aux, early_aux)
+    both, both_aux = join(early_mem, early_aux, late_mem, late_aux)
+    t_mem[...] = both.astype(jnp.bfloat16)
+    keep(t_aux, both_aux)
+
+    def plane_copies(step):
+        peer = {"sp": lax.rem(sp + 2 * step, ranks)}
+        return (
+            copy_to(t_mem, z_mem.at[step - 1], line_sems, (0, step - 1), peer),
+            copy_to(t_aux, z_aux.at[step - 1], line_sems, (1, step - 1), peer),
+        )
+
+    for step in range(1, depth):
+
+        @pl.when(row + step < depth)
+        def _():
+            for copy in plane_copies(step):
+                copy.start()
+
+    for kind in (0, 1):
+        for i in (3, 2, 1):
+            if (kind, i) != (0, 1):
+                z_weights(kind, i)
+    nearby(1, 1)
+    nearby(0, 2)
+    nearby(1, 2)
+
+    p_mem[...] = jnp.zeros(p_mem.shape, jnp.float32)
+    zero = jnp.zeros((1, DQK), jnp.float32)
+    keep(p_aux, (zero, jnp.full((1, DQK), LOWEST_LOG, jnp.float32), zero))
+    for step in range(depth - 1, 0, -1):
+
+        @pl.when(row >= step)
+        def _():
+            for copy in plane_copies(step):
+                copy.wait_recv()
+            memory, rest = join(
+                p_mem[...], parts(p_aux), z_mem[step - 1].astype(jnp.float32),
+                parts(z_aux.at[step - 1]),
+            )
+            p_mem[...] = memory
+            keep(p_aux, rest)
+
+    prior, prior_aux = p_mem[...], parts(p_aux)
+    more, more_aux = join(prior, prior_aux, e_mem[...], parts(e_aux))
+    q_mem[...] = pick(more, prior).astype(jnp.bfloat16)
+    keep(q_aux, tuple(pick(one, two) for one, two in zip(more_aux, prior_aux)))
+    send(q_mem, final_mem.at[col], state_sems, (2,), to_x)
+    send(q_aux, final_aux.at[col], state_sems, (3,), to_x)
+    x_weights(1)
+    final_mem[col] = pick(prior, more).astype(jnp.bfloat16)
+    keep(final_aux.at[col], tuple(pick(two, one) for one, two in zip(more_aux, prior_aux)))
+    pump(1)
+    loads["ogate"].wait()
+    loads["head"].wait()
+    arrived(final_mem.at[1 - col], state_sems, (2,))
+    arrived(final_aux.at[1 - col], state_sems, (3,))
+
+    for head in range(heads):
+        keys = slice(head * DQK, (head + 1) * DQK)
+        values = slice(head * DV, (head + 1) * DV)
+        prior_max = final_aux[head, 1:2, :]
+        start_max = jnp.maximum(final_aux[head, 2:3, :], prior_max)
+        lift = (jnp.exp(prior_max - start_max) * DQK ** (-0.5))[:, :1]
+        start_max = start_max[:, :1]
+        for at in range(3):
+            rows = slice(at * tile, (at + 1) * tile)
+            question = query[rows, keys]
+            found = cols[rows, 2 * heads + head : 2 * heads + head + 1]
+            carried = cols[rows, head : head + 1] + start_max
+            running = jnp.maximum(carried, found)
+            inside = jnp.exp(found - running)
+            scaled = jnp.exp(carried - running) * lift
+            numerator = inside * local[rows, values] + scaled * jnp.dot(
+                question, final_mem[head], preferred_element_type=jnp.float32
+            )
+            denominator = inside * cols[
+                rows, 3 * heads + head : 3 * heads + head + 1
+            ] + scaled * jnp.sum(
+                question.astype(jnp.float32) * final_aux[head, 0:1, :], axis=-1, keepdims=True
+            )
+            cell = numerator / jnp.maximum(jnp.abs(denominator), jnp.exp(-running))
+            centered = cell - jnp.mean(cell, axis=-1, keepdims=True)
+            cell = centered * lax.rsqrt(
+                jnp.mean(centered * centered, axis=-1, keepdims=True) + EPSILON
+            )
+            gate = ogate[rows, values].astype(jnp.float32)
+            gated[rows, values] = (
+                cell * head_gain[:, values] * jax.nn.sigmoid(gate)
+            ).astype(jnp.bfloat16)
+
+    def rows_of(owner):
+        return pl.ds(pl.multiple_of(owner * block, block), block)
+
+    send(gated.at[rows_of(corner), :], mate_gated.at[0], mate_sems, (0,), to_mate)
+    send(gated.at[rows_of(mate), :], mate_gated.at[1], mate_sems, (1,), to_mate)
+    loads["proj"].wait()
+    arrived(proj_mate, mate_sems, (2,))
+
+    def project(owner, slot, columns):
+        return jnp.dot(
+            gated[rows_of(owner), :], proj_own[:, columns], preferred_element_type=jnp.float32
+        ) + jnp.dot(
+            mate_gated[slot], proj_mate[:, columns], preferred_element_type=jnp.float32
+        )
+
+    arrived(mate_gated.at[0], mate_sems, (0,))
+    for at in range(count):
+        columns = slice(at * cols_out, (at + 1) * cols_out)
+        part_send[at] = project(across, 0, columns).astype(jnp.bfloat16)
+        send(part_send.at[at], part_recv.at[at], part_sems, (at,), to_y)
+    pump(1)
+    arrived(mate_gated.at[1], mate_sems, (1,))
+    for at in range(count):
+        columns = slice(at * cols_out, (at + 1) * cols_out)
+        acc[:, columns] = project(me, 1, columns)
+    pump(1)
+    for name in ("residual", "outg", "ing"):
+        loads[name].wait()
+    for at in range(count):
+        columns = slice(at * cols_out, (at + 1) * cols_out)
+        arrived(part_recv.at[at], part_sems, (at,))
+        acc[:, columns] = acc[:, columns] + part_recv[at].astype(jnp.float32)
+
+    member = lambda parity, owner: parity * count + owner
+    own = member(par, me)
+    cut = block // 2
+    for at in range(2):
+        rows = slice(at * cut, (at + 1) * cut)
+        mixed = acc[rows, :]
+        scale = lax.rsqrt(jnp.mean(mixed * mixed, axis=-1, keepdims=True) + EPSILON)
+        total = residual[rows, :].astype(jnp.float32) + mixed * scale * out_gain[...]
+        total = total.astype(jnp.bfloat16)
+        first_own[rows, :] = total
+        long = total.astype(jnp.float32)
+        scale = lax.rsqrt(jnp.mean(long * long, axis=-1, keepdims=True) + EPSILON)
+        normed[own, rows, :] = (long * scale * in_gain[...]).astype(jnp.bfloat16)
+        for slot, peer in ((0, to_mate), (1, to_y), (2, to_z)):
+            spot = normed.at[own, rows, :]
+            send(spot, spot, ag_sems, (slot, at), peer)
+    for slot, owner in ((0, mate), (1, across), (2, corner)):
+        columns = pl.ds(pl.multiple_of(owner * cols_out, cols_out), cols_out)
+        send(first_own.at[:, columns], first_cols.at[me], first_sems, (slot,), {"tp": owner})
+    columns = pl.ds(pl.multiple_of(me * cols_out, cols_out), cols_out)
+    first_cols[me] = first_own[:, columns]
+    x_weights(2)
+    for i in (3, 2, 1):
+        z_weights(2, i)
+
+    facing = 1 - par
+    came = {
+        0: member(par, mate), 1: member(par, across), 2: member(facing, me),
+        3: member(par, corner), 4: member(facing, mate), 5: member(facing, across),
+        6: member(facing, corner),
+    }
+
+    def take(slot, onward):
+        for at in range(2):
+            spot = normed.at[came[slot], at * cut : (at + 1) * cut, :]
+            arrived(spot, ag_sems, (slot, at))
+            for further, peer in onward:
+                send(spot, spot, ag_sems, (further, at), peer)
+
+    pump(3)
+    gathered(0)
+    gathered(1)
+
+    def mix(parity, at):
+        base = pl.multiple_of(parity * count + 2 * at, 2)
+        left_rows = normed[pl.ds(base, 2)].reshape(2 * block, width)
+        gate = jnp.dot(left_rows, gate_w[...], preferred_element_type=jnp.float32)
+        up = jnp.dot(left_rows, up_w[...], preferred_element_type=jnp.float32)
+        gate = (gate / (1.0 + jnp.exp(-gate)) * up).astype(jnp.bfloat16)
+        active[pl.ds(base, 2)] = gate.reshape(2, block, half)
+
+    take(1, [(3, to_mate)])
+    take(2, [(4, to_mate), (5, to_y)])
+    take(0, [])
+    mix(par, chip)
+    take(5, [(6, to_mate)])
+    take(3, [])
+    mix(par, 1 - chip)
+    pump(1)
+    take(4, [])
+    mix(facing, chip)
+    pump(1)
+    take(6, [])
+    mix(facing, 1 - chip)
+    pump(1)
+    gathered(2)
+
+    side = cols_out // 2
+
+    def term(parity, owner):
+        base = pl.multiple_of(parity * count, count)
+        left_rows = active[pl.ds(base, count)].reshape(rows_all, half)
+        return [
+            jnp.dot(left_rows, down_w[2 * owner + at], preferred_element_type=jnp.float32)
+            for at in range(2)
+        ]
+
+    targets = ((facing, 1 - chip), (par, 1 - chip), (facing, chip), (par, chip))
+
+    def for_mate(at):
+        parity, there = targets[at]
+        for piece_at, value_at in enumerate(term(parity, 2 * there + 1 - core)):
+            to_core[at, :, piece_at * side : (piece_at + 1) * side] = value_at.astype(
+                jnp.bfloat16
+            )
+        send(to_core.at[at], from_core.at[at], core_sems, (at,), to_mate)
+
+    def summed(at):
+        parity, there = targets[at]
+        low, top_part = term(parity, 2 * there + core)
+        arrived(from_core.at[at], core_sems, (at,))
+        return (
+            low + from_core[at, :, :side].astype(jnp.float32),
+            top_part + from_core[at, :, side:].astype(jnp.float32),
+        )
+
+    def pass_on(value_at, source, target, way, slot, peer):
+        source[slot] = value_at.astype(jnp.bfloat16)
+        send(source.at[slot], target.at[slot], link_sems, (way, slot), peer)
+
+    for_mate(0)
+    for_mate(1)
+    low, top_part = summed(0)
+    pass_on(low, y_send, y_recv, 0, 0, to_y)
+    pass_on(top_part, z_send, z_recv, 1, 0, to_z)
+    for_mate(2)
+    low, top_part = summed(1)
+    pass_on(low, y_send, y_recv, 0, 1, to_y)
+    held[0] = top_part
+    for_mate(3)
+    low, top_part = summed(2)
+    held[1] = low
+    pass_on(top_part, z_send, z_recv, 1, 1, to_z)
+    low, top_part = summed(3)
+    kept[:, :side] = low
+    kept[:, side:] = top_part
+    arrived(y_recv.at[0], link_sems, (0, 0))
+    pass_on(held[1] + y_recv[0].astype(jnp.float32), z_send, z_recv, 1, 2, to_z)
+    arrived(z_recv.at[0], link_sems, (1, 0))
+    pass_on(held[0] + z_recv[0].astype(jnp.float32), y_send, y_recv, 0, 2, to_y)
+    for slot, owner in ((0, mate), (1, across), (2, corner)):
+        arrived(first_cols.at[owner], first_sems, (slot,))
+    base_rows = first_cols[...].reshape(rows_all, cols_out).astype(jnp.float32)
+    arrived(y_recv.at[1], link_sems, (0, 1))
+    arrived(z_recv.at[1], link_sems, (1, 1))
+    kept[:, :side] = kept[:, :side] + y_recv[1].astype(jnp.float32)
+    kept[:, side:] = kept[:, side:] + z_recv[1].astype(jnp.float32)
+    arrived(z_recv.at[2], link_sems, (1, 2))
+    out_ref[:, :side] = (
+        base_rows[:, :side] + 0.5 * (kept[:, :side] + z_recv[2].astype(jnp.float32))
+    ).astype(jnp.bfloat16)
+    arrived(y_recv.at[2], link_sems, (0, 2))
+    out_ref[:, side:] = (
+        base_rows[:, side:] + 0.5 * (kept[:, side:] + y_recv[2].astype(jnp.float32))
+    ).astype(jnp.bfloat16)
+    for copy in sent:
+        copy.wait_send()
+    for step in range(1, depth):
+
+        @pl.when(row + step < depth)
+        def _():
+            for copy in plane_copies(step):
+                copy.wait_send()
+
+
+def paired(logs, cell_inputs, rows_inputs, weights):
+    ranks, count = lax.axis_size("sp"), lax.axis_size("tp")
+    heads = logs[0].shape[0]
+    residual, out_gain, in_gain = rows_inputs
+    projection, gate_weight, up_weight, down_weight = weights
+    rows, width = residual.shape
+    inner = projection.shape[0]
+    half = gate_weight.shape[1] // 2
+    cols = width // count
+    block, side, depth = rows // count, cols // 2, ranks // 2
+    dma = pltpu.SemaphoreType.DMA
+
+    def low(*shape):
+        return pltpu.VMEM(shape, jnp.bfloat16)
+
+    def full(*shape):
+        return pltpu.VMEM(shape, jnp.float32)
+
+    like = lambda array: pltpu.VMEM(array.shape, array.dtype)
+    members = 2 * count
+    operands = (*logs, *cell_inputs, residual, out_gain, in_gain, *weights)
+    return pl.pallas_call(
+        functools.partial(pair_kernel, ranks, count, heads),
+        out_shape=jax.ShapeDtypeStruct((rows, cols), jnp.bfloat16),
+        in_specs=[ANY] * len(operands),
+        out_specs=VMEM,
+        scratch_shapes=[
+            *(like(array) for array in (*logs, *cell_inputs)),
+            low(block, width), full(1, width), full(1, width),
+            low(inner, width), low(inner, width),
+            low(width, half), low(width, half), low(ranks, half, down_weight.shape[1]),
+            full(heads, rows), full(rows, 128),
+            full(heads, DQK, DV), low(heads, DQK, DV), full(heads, 8, DQK),
+            low(DQK, DV), full(8, DQK),
+            full(DQK, DV), full(8, DQK),
+            low(DQK, DV), full(8, DQK),
+            low(depth - 1, DQK, DV), full(depth - 1, 8, DQK),
+            full(DQK, DV), full(8, DQK),
+            low(DQK, DV), full(8, DQK),
+            low(heads, DQK, DV), full(heads, 8, DQK),
+            full(rows, inner), low(rows, inner), low(2, block, inner),
+            low(count, block, cols), low(count, block, cols), full(block, width),
+            low(block, width), low(count, block, cols),
+            low(members, block, width), low(members, block, half),
+            low(4, rows, cols), low(4, rows, cols),
+            low(3, rows, side), low(3, rows, side), low(3, rows, side), low(3, rows, side),
+            full(2, rows, side), full(rows, cols),
+            dma((15,)), dma((2, 3, 2, depth)), dma((2, 4)), dma((2, 2, depth - 1)), dma((2, 3)),
+            dma((2, count)), dma((2, 7, 2)), dma((2, 3)), dma((2, 4)), dma((2, 2, 3)),
+        ],
+        compiler_params=pltpu.CompilerParams(
+            collective_id=0, has_side_effects=True, vmem_limit_bytes=VMEM_BYTES
+        ),
+        name="layer",
+    )(*operands)
 
 
 def body(
@@ -494,6 +899,13 @@
     mixer_down_weight,
 ):
     heads_here = input_gate_log.shape[1]
+    if (lax.axis_size("sp"), lax.axis_size("tp"), heads_here) == (8, 4, 2):
+        return paired(
+            (forget_gate_logit.T, extra_head_decay.T, input_gate_log.T),
+            (query_matrix, key_matrix, value_matrix, output_gate_logit, head_norm_gain[None]),
+            (residual, cell_output_gain[None], mixer_input_gain[None]),
+            (projection, mixer_gate_weight, mixer_up_weight, mixer_down_weight),
+        )
     key_low = heads_first(key_matrix, heads_here, DQK)
     value_low = heads_first(value_matrix, heads_here, DV)
     keyed = key_low.astype(jnp.float32)

time: 212 us -> 182 us (0.86); the launches traced: 212 us -> 179 us
  Pallas kernels: 202 us -> 177 us
  local copies, waits for them, and re-layouts: 6.18 us -> 2.06 us
    pallas_call x1, Pallas kernels: 202 us -> 177 us  [paired(): pl.pallas_call(functools.partial(pair_kernel, ranks, count, heads), out_s...]
where the time goes in v1:
time: 182 us; the launch traced here: 179 us
  Pallas kernels  177 us (97%)
  local copies, waits for them, and re-layouts  2.06 us (1%)
    pallas_call x1, Pallas kernels, paired(): pl.pallas_call(functools.partial(pair_kernel, ranks, count, heads), out_s...  177 us

profile of v1, /device:TPU:25, one launch (start us, length us, event | category | flops | bytes accessed | tf_op | source)
XLA Modules:
  0.0 178.9 jit_solution(9904414861460914097)
XLA Ops:
  0.0 176.9 %layer.1 = bf16[768,512]{1,0:T(8,128)(2,1)} custom-call(f32[2,768]{1,0:T(2,128)} %bitcast.8, f32[2,768]{1,0:T(2,128)} %bitcast.9, f32[2,768]{1,0:T(2,128)} %bitcast.10, bf16[768,256]{1,0:T(8,128)(2,1)} %query_hbm.1, bf16[768,256]{1,0:T(8,128)(2,1)} %key_hbm.1, bf16[768,512]{1,0:T(8,128)(2,1)} %value_hbm.1, bf16[768,512]{1,0:T(8,128)(2,1)} %ogate_hbm.1, ...), custom_call_target="tpu_custom_call" | custom-call | tf_op jit(solution)/shard_map/layer/pallas_call | solution.py:848
  176.9 2.1 %copy.17 = bf16[768,512]{1,0:T(8,128)(2,1)} copy(bf16[768,512]{1,0:T(8,128)(2,1)} %layer.1) | data formatting | bytes 1572864

commit v2 on v1

--- a/solution.py
+++ b/solution.py
@@ -362,6 +362,7 @@
     half = gate_w.shape[1]
     high = gate_hbm.shape[0]
     others = {1: row + 1 - 2 * par, 2: lax.rem(row + 2, depth), 3: depth - 1 - row}
+    inner_row = jnp.logical_or(row == 1, row == 2)
     to_x = {"sp": row * 2 + 1 - col}
     to_z = {"sp": others[1] * 2 + col}
     to_mate, to_y = {"tp": mate}, {"tp": across}
@@ -418,32 +419,49 @@
     def arrived(target, sems, slot):
         copy_to(target, target, sems, slot, to_mate).wait_recv()
 
-    def z_weights(kind, i):
+    def z_copy(kind, i):
         there = others[i]
-        send(
+        return copy_to(
             piece(kind, lax.rem(there, 2)), place(kind, sp), w_sems, (kind, 0, i),
             {"sp": there * 2 + col},
         )
 
+    def z_weights(condition, *pieces):
+        @pl.when(condition)
+        def _():
+            for kind, i in pieces:
+                z_copy(kind, i).start()
+
     def x_weights(kind):
         send(piece(kind, par), place(kind, sp), w_sems, (kind, 1, 0), to_x)
 
-    relays = [(kind, i) for kind in range(3) for i in (1, 3, 2)]
+    relays = [(0, 1), (1, 1), (0, 3), (0, 2), (1, 3), (1, 2), (2, "soon"), (2, "late"), (2, 2)]
+    steps = {"soon": jnp.where(inner_row, 3, 1), "late": jnp.where(inner_row, 1, 3)}
+    others |= {
+        "soon": jnp.where(inner_row, others[3], others[1]),
+        "late": jnp.where(inner_row, others[1], others[3]),
+    }
 
     def pump(number):
         for _ in range(number):
             kind, i = relays.pop(0)
             spot = place(kind, others[i] * 2 + col)
-            arrived(spot, w_sems, (kind, 0, i))
-            send(spot, spot, w_sems, (kind, 1, i), to_x)
+            step = steps.get(i, i)
+            arrived(spot, w_sems, (kind, 0, step))
+            send(spot, spot, w_sems, (kind, 1, step), to_x)
 
     def gathered(kind):
-        loads[kind].wait()
         for i in range(depth):
             there = row if i == 0 else others[i]
             arrived(place(kind, there * 2 + 1 - col), w_sems, (kind, 1, i))
 
-    z_weights(0, 1)
+    odd, lower = par == 1, row < depth // 2
+    z_weights(row >= 0, (0, 1))
+    z_weights(row == 1, (0, 3))
+    z_weights(odd, (1, 1))
+    z_weights(jnp.logical_not(lower), (0, 3), (0, 2), (1, 3), (1, 2))
+    z_weights(row == 1, (2, 1))
+    z_weights(row == 2, (2, 3))
     send(projection_hbm, proj_mate, mate_sems, (2,), to_mate)
 
     for name in ("forget", "extra", "in"):
@@ -574,10 +592,11 @@
             for copy in plane_copies(step):
                 copy.start()
 
-    for kind in (0, 1):
-        for i in (3, 2, 1):
-            if (kind, i) != (0, 1):
-                z_weights(kind, i)
+    z_weights(par == 0, (1, 1))
+    z_weights(row == 0, (0, 3))
+    z_weights(lower, (0, 2), (1, 3), (1, 2))
+    z_weights(row == 2, (2, 1))
+    z_weights(row == 1, (2, 3))
     nearby(1, 1)
     nearby(0, 2)
     nearby(1, 2)
@@ -605,9 +624,9 @@
     send(q_mem, final_mem.at[col], state_sems, (2,), to_x)
     send(q_aux, final_aux.at[col], state_sems, (3,), to_x)
     x_weights(1)
+    x_weights(2)
     final_mem[col] = pick(prior, more).astype(jnp.bfloat16)
     keep(final_aux.at[col], tuple(pick(two, one) for one, two in zip(more_aux, prior_aux)))
-    pump(1)
     loads["ogate"].wait()
     loads["head"].wait()
     arrived(final_mem.at[1 - col], state_sems, (2,))
@@ -666,18 +685,19 @@
         columns = slice(at * cols_out, (at + 1) * cols_out)
         part_send[at] = project(across, 0, columns).astype(jnp.bfloat16)
         send(part_send.at[at], part_recv.at[at], part_sems, (at,), to_y)
-    pump(1)
     arrived(mate_gated.at[1], mate_sems, (1,))
     for at in range(count):
         columns = slice(at * cols_out, (at + 1) * cols_out)
         acc[:, columns] = project(me, 1, columns)
-    pump(1)
+    pump(2)
     for name in ("residual", "outg", "ing"):
         loads[name].wait()
     for at in range(count):
         columns = slice(at * cols_out, (at + 1) * cols_out)
         arrived(part_recv.at[at], part_sems, (at,))
         acc[:, columns] = acc[:, columns] + part_recv[at].astype(jnp.float32)
+        if at == 1:
+            pump(1)
 
     member = lambda parity, owner: parity * count + owner
     own = member(par, me)
@@ -695,14 +715,9 @@
         for slot, peer in ((0, to_mate), (1, to_y), (2, to_z)):
             spot = normed.at[own, rows, :]
             send(spot, spot, ag_sems, (slot, at), peer)
-    for slot, owner in ((0, mate), (1, across), (2, corner)):
-        columns = pl.ds(pl.multiple_of(owner * cols_out, cols_out), cols_out)
-        send(first_own.at[:, columns], first_cols.at[me], first_sems, (slot,), {"tp": owner})
+    z_weights(jnp.logical_not(inner_row), (2, 2), (2, 1), (2, 3))
     columns = pl.ds(pl.multiple_of(me * cols_out, cols_out), cols_out)
     first_cols[me] = first_own[:, columns]
-    x_weights(2)
-    for i in (3, 2, 1):
-        z_weights(2, i)
 
     facing = 1 - par
     came = {
@@ -711,14 +726,25 @@
         6: member(facing, corner),
     }
 
-    def take(slot, onward):
-        for at in range(2):
-            spot = normed.at[came[slot], at * cut : (at + 1) * cut, :]
-            arrived(spot, ag_sems, (slot, at))
-            for further, peer in onward:
-                send(spot, spot, ag_sems, (further, at), peer)
-
-    pump(3)
+    def take(slot, at, *onward):
+        spot = normed.at[came[slot], at * cut : (at + 1) * cut, :]
+        arrived(spot, ag_sems, (slot, at))
+        for further, peer in onward:
+            send(spot, spot, ag_sems, (further, at), peer)
+
+    pump(2)
+    take(1, 0, (3, to_mate))
+    take(2, 0, (4, to_mate), (5, to_y))
+    z_weights(inner_row, (2, 2))
+    take(1, 1, (3, to_mate))
+    pump(1)
+    take(2, 1, (4, to_mate), (5, to_y))
+    for slot, owner in ((0, mate), (1, across), (2, corner)):
+        columns = pl.ds(pl.multiple_of(owner * cols_out, cols_out), cols_out)
+        send(first_own.at[:, columns], first_cols.at[me], first_sems, (slot,), {"tp": owner})
+    pump(1)
+    for kind in range(3):
+        loads[kind].wait()
     gathered(0)
     gathered(1)
 
@@ -730,90 +756,105 @@
         gate = (gate / (1.0 + jnp.exp(-gate)) * up).astype(jnp.bfloat16)
         active[pl.ds(base, 2)] = gate.reshape(2, block, half)
 
-    take(1, [(3, to_mate)])
-    take(2, [(4, to_mate), (5, to_y)])
-    take(0, [])
+    take(0, 0)
+    take(0, 1)
     mix(par, chip)
-    take(5, [(6, to_mate)])
-    take(3, [])
+    take(5, 0, (6, to_mate))
+    take(3, 0)
+    take(3, 1)
     mix(par, 1 - chip)
-    pump(1)
-    take(4, [])
+    take(5, 1, (6, to_mate))
+    take(4, 0)
+    take(4, 1)
     mix(facing, chip)
     pump(1)
-    take(6, [])
+    take(6, 0)
+    take(6, 1)
     mix(facing, 1 - chip)
     pump(1)
-    gathered(2)
 
     side = cols_out // 2
-
-    def term(parity, owner):
+    slim = side // 2
+    targets = ((facing, 1 - chip), (par, 1 - chip), (facing, chip), (par, chip))
+
+    def term(stage, parity, owner):
         base = pl.multiple_of(parity * count, count)
         left_rows = active[pl.ds(base, count)].reshape(rows_all, half)
-        return [
-            jnp.dot(left_rows, down_w[2 * owner + at], preferred_element_type=jnp.float32)
-            for at in range(2)
-        ]
-
-    targets = ((facing, 1 - chip), (par, 1 - chip), (facing, chip), (par, chip))
-
-    def for_mate(at):
+        column = col if stage == 0 else 1 - col
+        return jnp.dot(
+            left_rows, down_w[2 * owner + column], preferred_element_type=jnp.float32
+        )
+
+    def for_mate(stage, at):
         parity, there = targets[at]
-        for piece_at, value_at in enumerate(term(parity, 2 * there + 1 - core)):
-            to_core[at, :, piece_at * side : (piece_at + 1) * side] = value_at.astype(
-                jnp.bfloat16
-            )
-        send(to_core.at[at], from_core.at[at], core_sems, (at,), to_mate)
-
-    def summed(at):
+        to_core[stage, at] = term(stage, parity, 2 * there + 1 - core).astype(jnp.bfloat16)
+        send(to_core.at[stage, at], from_core.at[stage, at], core_sems, (stage, at), to_mate)
+
+    def summed(stage, at):
         parity, there = targets[at]
-        low, top_part = term(parity, 2 * there + core)
-        arrived(from_core.at[at], core_sems, (at,))
-        return (
-            low + from_core[at, :, :side].astype(jnp.float32),
-            top_part + from_core[at, :, side:].astype(jnp.float32),
-        )
-
-    def pass_on(value_at, source, target, way, slot, peer):
-        source[slot] = value_at.astype(jnp.bfloat16)
-        send(source.at[slot], target.at[slot], link_sems, (way, slot), peer)
-
-    for_mate(0)
-    for_mate(1)
-    low, top_part = summed(0)
-    pass_on(low, y_send, y_recv, 0, 0, to_y)
-    pass_on(top_part, z_send, z_recv, 1, 0, to_z)
-    for_mate(2)
-    low, top_part = summed(1)
-    pass_on(low, y_send, y_recv, 0, 1, to_y)
-    held[0] = top_part
-    for_mate(3)
-    low, top_part = summed(2)
-    held[1] = low
-    pass_on(top_part, z_send, z_recv, 1, 1, to_z)
-    low, top_part = summed(3)
-    kept[:, :side] = low
-    kept[:, side:] = top_part
-    arrived(y_recv.at[0], link_sems, (0, 0))
-    pass_on(held[1] + y_recv[0].astype(jnp.float32), z_send, z_recv, 1, 2, to_z)
-    arrived(z_recv.at[0], link_sems, (1, 0))
-    pass_on(held[0] + z_recv[0].astype(jnp.float32), y_send, y_recv, 0, 2, to_y)
+        part = term(stage, parity, 2 * there + core)
+        arrived(from_core.at[stage, at], core_sems, (stage, at))
+        part = part + from_core[stage, at].astype(jnp.float32)
+        return part[:, :slim], part[:, slim:]
+
+    def pass_on(stage, value_at, source, target, way, slot, peer):
+        source[stage, slot] = value_at.astype(jnp.bfloat16)
+        send(source.at[stage, slot], target.at[stage, slot], link_sems, (way, stage, slot), peer)
+
+    def multiply(stage, between=lambda: None):
+        for_mate(stage, 0)
+        for_mate(stage, 1)
+        low, top_part = summed(stage, 0)
+        pass_on(stage, low, y_send, y_recv, 0, 0, to_y)
+        pass_on(stage, top_part, z_send, z_recv, 1, 0, to_z)
+        between()
+        for_mate(stage, 2)
+        low, top_part = summed(stage, 1)
+        pass_on(stage, low, y_send, y_recv, 0, 1, to_y)
+        held[stage, 0] = top_part
+        for_mate(stage, 3)
+        low, top_part = summed(stage, 2)
+        held[stage, 1] = low
+        pass_on(stage, top_part, z_send, z_recv, 1, 1, to_z)
+        low, top_part = summed(stage, 3)
+        kept[stage, :, :slim] = low
+        kept[stage, :, slim:] = top_part
+
+    def forward(stage):
+        arrived(y_recv.at[stage, 0], link_sems, (0, stage, 0))
+        pass_on(
+            stage, held[stage, 1] + y_recv[stage, 0].astype(jnp.float32), z_send, z_recv, 1, 2,
+            to_z,
+        )
+        arrived(z_recv.at[stage, 0], link_sems, (1, stage, 0))
+        pass_on(
+            stage, held[stage, 0] + z_recv[stage, 0].astype(jnp.float32), y_send, y_recv, 0, 2,
+            to_y,
+        )
+
+    def deliver(stage):
+        column = (col if stage == 0 else 1 - col) * side
+        for at, one, two in ((0, y_recv, z_recv), (1, z_recv, y_recv)):
+            way = at
+            arrived(one.at[stage, 1], link_sems, (way, stage, 1))
+            arrived(two.at[stage, 2], link_sems, (1 - way, stage, 2))
+            columns = pl.ds(pl.multiple_of(column + at * slim, slim), slim)
+            early = first_cols[:, :, columns].reshape(rows_all, slim).astype(jnp.float32)
+            whole = kept[stage, :, at * slim : (at + 1) * slim]
+            whole = whole + one[stage, 1].astype(jnp.float32) + two[stage, 2].astype(jnp.float32)
+            out_ref[:, columns] = (early + 0.5 * whole).astype(jnp.bfloat16)
+
+    multiply(0)
+    gathered(2)
+    multiply(1, lambda: forward(0))
+    forward(1)
     for slot, owner in ((0, mate), (1, across), (2, corner)):
         arrived(first_cols.at[owner], first_sems, (slot,))
-    base_rows = first_cols[...].reshape(rows_all, cols_out).astype(jnp.float32)
-    arrived(y_recv.at[1], link_sems, (0, 1))
-    arrived(z_recv.at[1], link_sems, (1, 1))
-    kept[:, :side] = kept[:, :side] + y_recv[1].astype(jnp.float32)
-    kept[:, side:] = kept[:, side:] + z_recv[1].astype(jnp.float32)
-    arrived(z_recv.at[2], link_sems, (1, 2))
-    out_ref[:, :side] = (
-        base_rows[:, :side] + 0.5 * (kept[:, :side] + z_recv[2].astype(jnp.float32))
-    ).astype(jnp.bfloat16)
-    arrived(y_recv.at[2], link_sems, (0, 2))
-    out_ref[:, side:] = (
-        base_rows[:, side:] + 0.5 * (kept[:, side:] + y_recv[2].astype(jnp.float32))
-    ).astype(jnp.bfloat16)
+    deliver(0)
+    deliver(1)
+    for kind in range(3):
+        for i in (1, 2, 3):
+            z_copy(kind, i).wait_send()
     for copy in sent:
         copy.wait_send()
     for step in range(1, depth):
@@ -868,11 +909,11 @@
             low(count, block, cols), low(count, block, cols), full(block, width),
             low(block, width), low(count, block, cols),
             low(members, block, width), low(members, block, half),
-            low(4, rows, cols), low(4, rows, cols),
-            low(3, rows, side), low(3, rows, side), low(3, rows, side), low(3, rows, side),
-            full(2, rows, side), full(rows, cols),
+            low(2, 4, rows, side), low(2, 4, rows, side),
+            *(low(2, 3, rows, side // 2) for _ in range(4)),
+            full(2, 2, rows, side // 2), full(2, rows, side),
             dma((15,)), dma((2, 3, 2, depth)), dma((2, 4)), dma((2, 2, depth - 1)), dma((2, 3)),
-            dma((2, count)), dma((2, 7, 2)), dma((2, 3)), dma((2, 4)), dma((2, 2, 3)),
+            dma((2, count)), dma((2, 7, 2)), dma((2, 3)), dma((2, 2, 4)), dma((2, 2, 2, 3)),
         ],
         compiler_params=pltpu.CompilerParams(
             collective_id=0, has_side_effects=True, vmem_limit_bytes=VMEM_BYTES

time: 182 us -> 132 us (0.73); the launches traced: 179 us -> 132 us
  Pallas kernels: 177 us -> 130 us
    pallas_call x1, Pallas kernels: 177 us -> 130 us  [paired(): pl.pallas_call(functools.partial(pair_kernel, ranks, count, heads), out_s...]
where the time goes in v2:
time: 132 us
  Pallas kernels  130 us (98%)
  local copies, waits for them, and re-layouts  2.06 us (2%)
    pallas_call x1, Pallas kernels, paired(): pl.pallas_call(functools.partial(pair_kernel, ranks, count, heads), out_s...  130 us

profile of v2, /device:TPU:25, one launch (start us, length us, event | category | flops | bytes accessed | tf_op | source)
XLA Modules:
  0.0 131.6 jit_solution(2071992275624986875)
XLA Ops:
  0.0 129.5 %layer.1 = bf16[768,512]{1,0:T(8,128)(2,1)} custom-call(f32[2,768]{1,0:T(2,128)} %bitcast.8, f32[2,768]{1,0:T(2,128)} %bitcast.9, f32[2,768]{1,0:T(2,128)} %bitcast.10, bf16[768,256]{1,0:T(8,128)(2,1)} %query_hbm.1, bf16[768,256]{1,0:T(8,128)(2,1)} %key_hbm.1, bf16[768,512]{1,0:T(8,128)(2,1)} %value_hbm.1, bf16[768,512]{1,0:T(8,128)(2,1)} %ogate_hbm.1, ...), custom_call_target="tpu_custom_call" | custom-call | tf_op jit(solution)/shard_map/layer/pallas_call | solution.py:889
  129.5 2.1 %copy.17 = bf16[768,512]{1,0:T(8,128)(2,1)} copy(bf16[768,512]{1,0:T(8,128)(2,1)} %layer.1) | data formatting | bytes 1572864

commit v3 on v2

--- a/solution.py
+++ b/solution.py
@@ -343,7 +343,7 @@
     out_gain, in_gain, proj_own, proj_mate, gate_w, up_w, down_w, cum_row, cols, own_mem, mem_send,
     aux, x_mem, x_aux, e_mem, e_aux, t_mem, t_aux, z_mem, z_aux, p_mem, p_aux, q_mem, q_aux,
     final_mem, final_aux, local, gated, mate_gated, part_send, part_recv, acc, first_own,
-    first_cols, normed, active, to_core, from_core, y_send, y_recv, z_send, z_recv, held, kept,
+    first_cols, normed, active, to_core, from_core, y_send, y_recv, z_send, z_recv, ours, held, kept, result,
     local_sems, w_sems, state_sems, line_sems, mate_sems, part_sems, ag_sems, first_sems,
     core_sems, link_sems,
 ):
@@ -360,6 +360,7 @@
     cols_out = out_ref.shape[1]
     block = rows_all // count
     half = gate_w.shape[1]
+    quarter = half // 2
     high = gate_hbm.shape[0]
     others = {1: row + 1 - 2 * par, 2: lax.rem(row + 2, depth), 3: depth - 1 - row}
     inner_row = jnp.logical_or(row == 1, row == 2)
@@ -395,18 +396,19 @@
     load("ing", in_gain_hbm, in_gain)
 
     def piece(kind, parity):
+        if kind >= 2:
+            start = parity * half + (kind - 2) * quarter
+            return down_hbm.at[pl.ds(pl.multiple_of(start, quarter), quarter), :]
         at = pl.ds(pl.multiple_of(parity * half, half), half)
-        if kind == 2:
-            return down_hbm.at[at, :]
         return (gate_hbm, up_hbm)[kind].at[:, at]
 
     def place(kind, owner):
-        if kind == 2:
-            return down_w.at[owner]
+        if kind >= 2:
+            return down_w.at[owner, (kind - 2) * quarter : (kind - 1) * quarter, :]
         at = pl.ds(pl.multiple_of(owner * high, high), high)
         return (gate_w, up_w)[kind].at[at, :]
 
-    for kind in range(3):
+    for kind in range(4):
         load(kind, piece(kind, par), place(kind, sp))
 
     pl.semaphore_wait(barrier, len(greeted))
@@ -435,7 +437,8 @@
     def x_weights(kind):
         send(piece(kind, par), place(kind, sp), w_sems, (kind, 1, 0), to_x)
 
-    relays = [(0, 1), (1, 1), (0, 3), (0, 2), (1, 3), (1, 2), (2, "soon"), (2, "late"), (2, 2)]
+    relays = [(0, 1), (1, 1), (0, 3), (0, 2), (1, 3), (1, 2), (2, "soon"), (3, "soon")]
+    relays += [(2, "late"), (3, "late"), (2, 2), (3, 2)]
     steps = {"soon": jnp.where(inner_row, 3, 1), "late": jnp.where(inner_row, 1, 3)}
     others |= {
         "soon": jnp.where(inner_row, others[3], others[1]),
@@ -460,8 +463,8 @@
     z_weights(row == 1, (0, 3))
     z_weights(odd, (1, 1))
     z_weights(jnp.logical_not(lower), (0, 3), (0, 2), (1, 3), (1, 2))
-    z_weights(row == 1, (2, 1))
-    z_weights(row == 2, (2, 3))
+    z_weights(row == 1, (2, 1), (3, 1))
+    z_weights(row == 2, (2, 3), (3, 3))
     send(projection_hbm, proj_mate, mate_sems, (2,), to_mate)
 
     for name in ("forget", "extra", "in"):
@@ -585,7 +588,7 @@
             copy_to(t_aux, z_aux.at[step - 1], line_sems, (1, step - 1), peer),
         )
 
-    for step in range(1, depth):
+    for step in range(depth - 1, 0, -1):
 
         @pl.when(row + step < depth)
         def _():
@@ -595,8 +598,8 @@
     z_weights(par == 0, (1, 1))
     z_weights(row == 0, (0, 3))
     z_weights(lower, (0, 2), (1, 3), (1, 2))
-    z_weights(row == 2, (2, 1))
-    z_weights(row == 1, (2, 3))
+    z_weights(row == 2, (2, 1), (3, 1))
+    z_weights(row == 1, (2, 3), (3, 3))
     nearby(1, 1)
     nearby(0, 2)
     nearby(1, 2)
@@ -625,6 +628,7 @@
     send(q_aux, final_aux.at[col], state_sems, (3,), to_x)
     x_weights(1)
     x_weights(2)
+    x_weights(3)
     final_mem[col] = pick(prior, more).astype(jnp.bfloat16)
     keep(final_aux.at[col], tuple(pick(two, one) for one, two in zip(more_aux, prior_aux)))
     loads["ogate"].wait()
@@ -689,14 +693,14 @@
     for at in range(count):
         columns = slice(at * cols_out, (at + 1) * cols_out)
         acc[:, columns] = project(me, 1, columns)
-    pump(2)
+    pump(1)
     for name in ("residual", "outg", "ing"):
         loads[name].wait()
     for at in range(count):
         columns = slice(at * cols_out, (at + 1) * cols_out)
         arrived(part_recv.at[at], part_sems, (at,))
         acc[:, columns] = acc[:, columns] + part_recv[at].astype(jnp.float32)
-        if at == 1:
+        if at < 2:
             pump(1)
 
     member = lambda parity, owner: parity * count + owner
@@ -715,7 +719,7 @@
         for slot, peer in ((0, to_mate), (1, to_y), (2, to_z)):
             spot = normed.at[own, rows, :]
             send(spot, spot, ag_sems, (slot, at), peer)
-    z_weights(jnp.logical_not(inner_row), (2, 2), (2, 1), (2, 3))
+    z_weights(jnp.logical_not(inner_row), (2, 2), (3, 2), (2, 1), (3, 1), (2, 3), (3, 3))
     columns = pl.ds(pl.multiple_of(me * cols_out, cols_out), cols_out)
     first_cols[me] = first_own[:, columns]
 
@@ -735,15 +739,14 @@
     pump(2)
     take(1, 0, (3, to_mate))
     take(2, 0, (4, to_mate), (5, to_y))
-    z_weights(inner_row, (2, 2))
+    z_weights(inner_row, (2, 2), (3, 2))
     take(1, 1, (3, to_mate))
     pump(1)
     take(2, 1, (4, to_mate), (5, to_y))
     for slot, owner in ((0, mate), (1, across), (2, corner)):
         columns = pl.ds(pl.multiple_of(owner * cols_out, cols_out), cols_out)
         send(first_own.at[:, columns], first_cols.at[me], first_sems, (slot,), {"tp": owner})
-    pump(1)
-    for kind in range(3):
+    for kind in range(4):
         loads[kind].wait()
     gathered(0)
     gathered(1)
@@ -763,15 +766,15 @@
     take(3, 0)
     take(3, 1)
     mix(par, 1 - chip)
-    take(5, 1, (6, to_mate))
+    pump(2)
     take(4, 0)
     take(4, 1)
     mix(facing, chip)
-    pump(1)
+    take(5, 1, (6, to_mate))
     take(6, 0)
     take(6, 1)
     mix(facing, 1 - chip)
-    pump(1)
+    pump(4)
 
     side = cols_out // 2
     slim = side // 2
@@ -785,34 +788,32 @@
             left_rows, down_w[2 * owner + column], preferred_element_type=jnp.float32
         )
 
-    def for_mate(stage, at):
+    def both(stage, at):
         parity, there = targets[at]
         to_core[stage, at] = term(stage, parity, 2 * there + 1 - core).astype(jnp.bfloat16)
+        ours[at] = term(stage, parity, 2 * there + core)
         send(to_core.at[stage, at], from_core.at[stage, at], core_sems, (stage, at), to_mate)
 
     def summed(stage, at):
-        parity, there = targets[at]
-        part = term(stage, parity, 2 * there + core)
         arrived(from_core.at[stage, at], core_sems, (stage, at))
-        part = part + from_core[stage, at].astype(jnp.float32)
+        part = ours[at] + from_core[stage, at].astype(jnp.float32)
         return part[:, :slim], part[:, slim:]
 
     def pass_on(stage, value_at, source, target, way, slot, peer):
         source[stage, slot] = value_at.astype(jnp.bfloat16)
         send(source.at[stage, slot], target.at[stage, slot], link_sems, (way, stage, slot), peer)
 
-    def multiply(stage, between=lambda: None):
-        for_mate(stage, 0)
-        for_mate(stage, 1)
+    def multiply(stage):
+        both(stage, 0)
+        both(stage, 1)
         low, top_part = summed(stage, 0)
         pass_on(stage, low, y_send, y_recv, 0, 0, to_y)
         pass_on(stage, top_part, z_send, z_recv, 1, 0, to_z)
-        between()
-        for_mate(stage, 2)
+        both(stage, 2)
         low, top_part = summed(stage, 1)
         pass_on(stage, low, y_send, y_recv, 0, 1, to_y)
         held[stage, 0] = top_part
-        for_mate(stage, 3)
+        both(stage, 3)
         low, top_part = summed(stage, 2)
         held[stage, 1] = low
         pass_on(stage, top_part, z_send, z_recv, 1, 1, to_z)
@@ -842,27 +843,41 @@
             early = first_cols[:, :, columns].reshape(rows_all, slim).astype(jnp.float32)
             whole = kept[stage, :, at * slim : (at + 1) * slim]
             whole = whole + one[stage, 1].astype(jnp.float32) + two[stage, 2].astype(jnp.float32)
-            out_ref[:, columns] = (early + 0.5 * whole).astype(jnp.bfloat16)
-
+            result[:, columns] = (early + 0.5 * whole).astype(jnp.bfloat16)
+            written = pltpu.make_async_copy(
+                result.at[:, columns], out_ref.at[:, columns], local_sems.at[16 + 2 * stage + at]
+            )
+            written.start()
+            writes.append(written)
+
+    before = len(sent)
     multiply(0)
+    forward(0)
     gathered(2)
-    multiply(1, lambda: forward(0))
+    gathered(3)
+    multiply(1)
     forward(1)
     for slot, owner in ((0, mate), (1, across), (2, corner)):
         arrived(first_cols.at[owner], first_sems, (slot,))
-    deliver(0)
-    deliver(1)
-    for kind in range(3):
+    writes = []
+    for kind in range(4):
         for i in (1, 2, 3):
             z_copy(kind, i).wait_send()
-    for copy in sent:
-        copy.wait_send()
     for step in range(1, depth):
 
         @pl.when(row + step < depth)
         def _():
             for copy in plane_copies(step):
                 copy.wait_send()
+
+    for copy in sent[:before]:
+        copy.wait_send()
+    deliver(0)
+    deliver(1)
+    for copy in sent[before:]:
+        copy.wait_send()
+    for copy in writes:
+        copy.wait()
 
 
 def paired(logs, cell_inputs, rows_inputs, weights):
@@ -890,7 +905,7 @@
         functools.partial(pair_kernel, ranks, count, heads),
         out_shape=jax.ShapeDtypeStruct((rows, cols), jnp.bfloat16),
         in_specs=[ANY] * len(operands),
-        out_specs=VMEM,
+        out_specs=ANY,
         scratch_shapes=[
             *(like(array) for array in (*logs, *cell_inputs)),
             low(block, width), full(1, width), full(1, width),
@@ -911,8 +926,9 @@
             low(members, block, width), low(members, block, half),
             low(2, 4, rows, side), low(2, 4, rows, side),
             *(low(2, 3, rows, side // 2) for _ in range(4)),
-            full(2, 2, rows, side // 2), full(2, rows, side),
-            dma((15,)), dma((2, 3, 2, depth)), dma((2, 4)), dma((2, 2, depth - 1)), dma((2, 3)),
+            full(4, rows, side), full(2, 2, rows, side // 2), full(2, rows, side),
+            low(rows, cols),
+            dma((20,)), dma((2, 4, 2, depth)), dma((2, 4)), dma((2, 2, depth - 1)), dma((2, 3)),
             dma((2, count)), dma((2, 7, 2)), dma((2, 3)), dma((2, 2, 4)), dma((2, 2, 2, 3)),
         ],
         compiler_params=pltpu.CompilerParams(

time: 132 us -> 129 us (0.977)
  Pallas kernels: 130 us -> 127 us
    pallas_call x1, Pallas kernels: 130 us -> 127 us  [paired(): pl.pallas_call(functools.partial(pair_kernel, ranks, count, heads), out_s...]
where the time goes in v3:
time: 129 us
  Pallas kernels  127 us (98%)
  local copies, waits for them, and re-layouts  2.06 us (2%)
    pallas_call x1, Pallas kernels, paired(): pl.pallas_call(functools.partial(pair_kernel, ranks, count, heads), out_s...  127 us

profile of v3, /device:TPU:25, one launch (start us, length us, event | category | flops | bytes accessed | tf_op | source)
XLA Modules:
  0.0 128.8 jit_solution(2393528589534061142)
XLA Ops:
  0.0 126.7 %layer.1 = bf16[768,512]{1,0:T(8,128)(2,1)} custom-call(f32[2,768]{1,0:T(2,128)} %bitcast.8, f32[2,768]{1,0:T(2,128)} %bitcast.9, f32[2,768]{1,0:T(2,128)} %bitcast.10, bf16[768,256]{1,0:T(8,128)(2,1)} %query_hbm.1, bf16[768,256]{1,0:T(8,128)(2,1)} %key_hbm.1, bf16[768,512]{1,0:T(8,128)(2,1)} %value_hbm.1, bf16[768,512]{1,0:T(8,128)(2,1)} %ogate_hbm.1, ...), custom_call_target="tpu_custom_call" | custom-call | tf_op jit(solution)/shard_map/layer/pallas_call | solution.py:904
  126.7 2.1 %copy.17 = bf16[768,512]{1,0:T(8,128)(2,1)} copy(bf16[768,512]{1,0:T(8,128)(2,1)} %layer.1) | data formatting | bytes 1572864

commit v4 on v3

--- a/solution.py
+++ b/solution.py
@@ -345,7 +345,7 @@
     final_mem, final_aux, local, gated, mate_gated, part_send, part_recv, acc, first_own,
     first_cols, normed, active, to_core, from_core, y_send, y_recv, z_send, z_recv, ours, held, kept, result,
     local_sems, w_sems, state_sems, line_sems, mate_sems, part_sems, ag_sems, first_sems,
-    core_sems, link_sems,
+    core_sems, link_sems, out_sems,
 ):
     sp, me = lax.axis_index("sp"), lax.axis_index("tp")
     row, col = sp // 2, lax.rem(sp, 2)
@@ -368,6 +368,25 @@
     to_z = {"sp": others[1] * 2 + col}
     to_mate, to_y = {"tp": mate}, {"tp": across}
     sent = []
+    lanes = {
+        id(w_sems): lambda slot: 3 * slot[1] + min(slot[0], 2), id(ag_sems): lambda slot: 6,
+        id(part_sems): lambda slot: 7, id(core_sems): lambda slot: 8,
+        id(link_sems): lambda slot: 9 + slot[0],
+    }
+
+    def outward(source, target, sems, slot, peer):
+        if id(sems) not in lanes:
+            return copy_to(source, target, sems, slot, peer)
+        return pltpu.make_async_remote_copy(
+            source, target, out_sems.at[lanes[id(sems)](slot)], sems.at[slot], device_id=peer,
+            device_id_type=MESH,
+        )
+
+    def all_left(lane, whole):
+        lane = out_sems.at[lane]
+        pltpu.make_async_remote_copy(
+            whole, whole, lane, lane, device_id=to_mate, device_id_type=MESH
+        ).wait_send()
 
     barrier = pltpu.get_barrier_semaphore()
     greeted = [{"sp": others[i] * 2 + col} for i in (1, 2, 3)]
@@ -414,16 +433,17 @@
     pl.semaphore_wait(barrier, len(greeted))
 
     def send(source, target, sems, slot, peer):
-        copy = copy_to(source, target, sems, slot, peer)
+        copy = outward(source, target, sems, slot, peer)
         copy.start()
-        sent.append(copy)
+        if id(sems) not in lanes:
+            sent.append(copy)
 
     def arrived(target, sems, slot):
-        copy_to(target, target, sems, slot, to_mate).wait_recv()
+        outward(target, target, sems, slot, to_mate).wait_recv()
 
     def z_copy(kind, i):
         there = others[i]
-        return copy_to(
+        return outward(
             piece(kind, lax.rem(there, 2)), place(kind, sp), w_sems, (kind, 0, i),
             {"sp": there * 2 + col},
         )
@@ -850,7 +870,6 @@
             written.start()
             writes.append(written)
 
-    before = len(sent)
     multiply(0)
     forward(0)
     gathered(2)
@@ -860,9 +879,12 @@
     for slot, owner in ((0, mate), (1, across), (2, corner)):
         arrived(first_cols.at[owner], first_sems, (slot,))
     writes = []
-    for kind in range(4):
-        for i in (1, 2, 3):
-            z_copy(kind, i).wait_send()
+    for lane, count_out in ((0, depth - 1), (3, depth)):
+        all_left(lane, gate_w.at[: count_out * high, :])
+        all_left(lane + 1, up_w.at[: count_out * high, :])
+        all_left(lane + 2, down_w.at[:count_out])
+    all_left(6, normed.at[:7])
+    all_left(7, part_send)
     for step in range(1, depth):
 
         @pl.when(row + step < depth)
@@ -870,12 +892,12 @@
             for copy in plane_copies(step):
                 copy.wait_send()
 
-    for copy in sent[:before]:
+    for copy in sent:
         copy.wait_send()
     deliver(0)
     deliver(1)
-    for copy in sent[before:]:
-        copy.wait_send()
+    for lane, whole in ((8, to_core), (9, y_send), (10, z_send)):
+        all_left(lane, whole)
     for copy in writes:
         copy.wait()
 
@@ -928,8 +950,8 @@
             *(low(2, 3, rows, side // 2) for _ in range(4)),
             full(4, rows, side), full(2, 2, rows, side // 2), full(2, rows, side),
             low(rows, cols),
-            dma((20,)), dma((2, 4, 2, depth)), dma((2, 4)), dma((2, 2, depth - 1)), dma((2, 3)),
-            dma((2, count)), dma((2, 7, 2)), dma((2, 3)), dma((2, 2, 4)), dma((2, 2, 2, 3)),
+            dma((20,)), dma((4, 2, depth)), dma((2, 4)), dma((2, 2, depth - 1)), dma((2, 3)),
+            dma((count,)), dma((7, 2)), dma((2, 3)), dma((2, 4)), dma((2, 2, 3)), dma((11,)),
         ],
         compiler_params=pltpu.CompilerParams(
             collective_id=0, has_side_effects=True, vmem_limit_bytes=VMEM_BYTES

time: 129 us -> 129 us (level)
  no operation moved by 1% of the time
where the time goes in v4:
time: 129 us; the launch traced here: 128 us
  Pallas kernels  126 us (98%)
  local copies, waits for them, and re-layouts  2.06 us (2%)
    pallas_call x1, Pallas kernels, paired(): pl.pallas_call(functools.partial(pair_kernel, ranks, count, heads), out_s...  126 us

profile of v4, /device:TPU:25, one launch (start us, length us, event | category | flops | bytes accessed | tf_op | source)
XLA Modules:
  0.0 128.3 jit_solution(15463983830448993647)
XLA Ops:
  0.0 126.2 %layer.1 = bf16[768,512]{1,0:T(8,128)(2,1)} custom-call(f32[2,768]{1,0:T(2,128)} %bitcast.8, f32[2,768]{1,0:T(2,128)} %bitcast.9, f32[2,768]{1,0:T(2,128)} %bitcast.10, bf16[768,256]{1,0:T(8,128)(2,1)} %query_hbm.1, bf16[768,256]{1,0:T(8,128)(2,1)} %key_hbm.1, bf16[768,512]{1,0:T(8,128)(2,1)} %value_hbm.1, bf16[768,512]{1,0:T(8,128)(2,1)} %ogate_hbm.1, ...), custom_call_target="tpu_custom_call" | custom-call | tf_op jit(solution)/shard_map/layer/pallas_call | solution.py:926
  126.2 2.1 %copy.17 = bf16[768,512]{1,0:T(8,128)(2,1)} copy(bf16[768,512]{1,0:T(8,128)(2,1)} %layer.1) | data formatting | bytes 1572864
